TPU v7x, 1024 devices: a whole 8x8x8 slice. The times are simulated.
1024 devices in a mesh: tp: 64 (over z, y), dp: 16 (over x, core).
Axes of the slice: x: 8, y: 8, z: 8, core: 2. Of those that a mesh axis runs over, the one named last changes fastest.
Arguments:
- tokens: bfloat16 [256, 4096], P('tp', 'dp'), may hold values from -30 to 30
- lengths: int32 [256], P('dp'), may hold values from 1 to 2048, 65536 in all
- states: float32 [2, 256, 2048, 128], P(None, 'dp', 'tp'), may hold values from -0.8 to 0.8
- norm_gain: bfloat16 [2, 4096], P(None, 'dp'), may hold values from 0.099609375 to 1.8984375
- w_query: bfloat16 [2, 4096, 2048], P(None, 'dp', 'tp'), may hold values from -0.09375 to 0.09375
- w_key: bfloat16 [2, 4096, 2048], P(None, 'dp', 'tp'), may hold values from -0.09375 to 0.09375
- w_value: bfloat16 [2, 4096, 2048], P(None, 'dp', 'tp'), may hold values from -0.09375 to 0.09375
- w_gate: bfloat16 [2, 4096, 2048], P(None, 'dp', 'tp'), may hold values from -0.09375 to 0.09375
- head_gain: bfloat16 [2, 2048], P(None, 'tp'), may hold values from 0.099609375 to 1.8984375
- w_out: bfloat16 [2, 2048, 4096], P(None, 'tp', 'dp'), may hold values from -0.125 to 0.125
Outputs:
- hidden_out: bfloat16 [256, 4096], P('tp', 'dp')
- new_states: float32 [2, 256, 2048, 128], P(None, 'dp', 'tp')
All inputs are finite; a program needn't handle non-finite values. No bound on the sum of `lengths` on one device may be relied on, other than what follows from the above.
Results may differ from a plain program's by a relative error of at most 0.012.
Values may be sent and summed in bfloat16 or wider, within the bound.
A program may use at most 32 MiB of HBM per device.

v0:
```python
import math

import jax
import jax.numpy as jnp
from jax import lax
from jax.sharding import PartitionSpec as P

D = 4096
HEADS = 16
DK = 128
LAYERS = 2


norm_eps = 1e-06
group_eps = 1e-05
rotary_base = 10000.0


def partner_2(value, axis, apart):
    mask = 2**apart
    pairs = [(source, source ^ mask) for source in range(lax.axis_size(axis))]
    return lax.ppermute(value, axis, pairs)


def sent_to_all(shard, axis):
    copies = jnp.broadcast_to(shard, (lax.axis_size(axis), *shard.shape))
    return lax.all_to_all(copies, axis, split_axis=0, concat_axis=0, tiled=True)


def joined_along(blocks, dim):
    blocks = jnp.moveaxis(blocks, 0, dim)
    lengths = blocks.shape
    return blocks.reshape(*lengths[:dim], lengths[dim] * lengths[dim + 1], *lengths[dim + 2 :])


def collect(shard, axis, dim):
    blocks = sent_to_all(shard, axis)
    return joined_along(blocks, dim)


def cut_along(shard, dim, count):
    lengths = shard.shape
    blocks = shard.reshape(*lengths[:dim], count, lengths[dim] // count, *lengths[dim + 1 :])
    return jnp.moveaxis(blocks, dim, 0)


def summed_on_arrival(shard, axis, dim):
    count = lax.axis_size(axis)
    blocks = lax.all_to_all(cut_along(shard, dim, count), axis, 0, 0, tiled=True)
    return jnp.sum(blocks, axis=0)


def side_by_side(arrays, axis, dim, along):
    widths = [math.prod(a.shape[along:]) for a in arrays]
    both = jnp.concatenate(
        [a.reshape(*a.shape[:along], w) for a, w in zip(arrays, widths)], axis=along
    )
    result = summed_on_arrival(both, axis, dim)
    blocks = jnp.split(result, [sum(widths[:k]) for k in range(1, len(widths))], axis=along)
    return tuple(
        (b.reshape(*result.shape[:along], *a.shape[along:]) for a, b in zip(arrays, blocks))
    )


def rotate(values, positions):
    half_size = values.shape[-1] // 2
    inverse = rotary_base ** (-jnp.arange(half_size, dtype=jnp.float32) / half_size)
    angles = positions.astype(jnp.float32)[:, None] * inverse[None, :]
    cosine = jnp.cos(angles)[:, None, :]
    sine_v = jnp.sin(angles)[:, None, :]
    first_part = values[..., :half_size]
    second = values[..., half_size:]
    return jnp.concatenate(
        [first_part * cosine - second * sine_v, first_part * sine_v + second * cosine], axis=-1
    )


def decays(head_ids):
    return 1.0 - jnp.exp2(-1.0 - 9.0 * head_ids.astype(jnp.float32) / (HEADS - 1))


def body(tokens, lengths, states, norm_gain, w_query, w_key, w_value, w_gate, head_gain, w_out):
    tp_index = lax.axis_index("tp")
    columns = w_query.shape[2]
    pieces = max(DK // columns, 1)
    levels = pieces.bit_length() - 1
    local_heads = max(columns // DK, 1)
    value_cols = columns // local_heads
    head_ids = tp_index * columns // DK + jnp.arange(local_heads, dtype=jnp.int32)
    gammas = decays(head_ids)
    hidden_x = tokens
    outputs = []
    for layer_id in range(LAYERS):
        prior_state = states[layer_id]
        row_total = prior_state.shape[0]
        x_float = hidden_x.astype(jnp.float32)
        feature_gain = norm_gain[layer_id].astype(jnp.float32)
        weights = jnp.concatenate(
            [w_query[layer_id], w_key[layer_id], w_value[layer_id], w_gate[layer_id]], axis=1
        )
        gathered = collect(hidden_x, "tp", 0)
        gathered_f = gathered.astype(jnp.float32)
        normed = (gathered_f * feature_gain).astype(jnp.bfloat16)
        partial_value = jnp.dot(normed, weights, preferred_element_type=jnp.float32)
        summed, own_squares = side_by_side(
            (partial_value, jnp.sum(gathered_f * gathered_f, axis=1)), "dp", 0, 1
        )
        row_scale = lax.rsqrt(own_squares / D + norm_eps)
        projected = (summed * row_scale[:, None]).astype(jnp.bfloat16)
        query_rows = projected[:, :columns]
        key_rows = projected[:, columns : 2 * columns]
        value_rows = projected[:, 2 * columns : 3 * columns]
        gate_rows = projected[:, 3 * columns :]
        stacked = jnp.stack([query_rows, key_rows])
        for join_level_id in range(levels):
            partner = partner_2(stacked, "tp", join_level_id)
            upper_bit = tp_index // 2**join_level_id % 2
            stacked = jnp.where(
                upper_bit == 1,
                jnp.concatenate([partner, stacked], axis=-1),
                jnp.concatenate([stacked, partner], axis=-1),
            )
        query_f = rotate(
            stacked[0].astype(jnp.float32).reshape(row_total, local_heads, DK), lengths
        )
        key_f = rotate(
            stacked[1].astype(jnp.float32).reshape(row_total, local_heads, DK), lengths
        ) * DK ** (-0.5)
        values_f = value_rows.astype(jnp.float32).reshape(row_total, local_heads, value_cols)
        state_view = prior_state.reshape(row_total, local_heads, value_cols, DK)
        updated = gammas[None, :, None, None] * state_view + jnp.einsum(
            "shd,shv->shvd", key_f, values_f
        )
        readout = jnp.einsum("shd,shvd->shv", query_f, updated)
        head_stats = jnp.stack([jnp.sum(readout, axis=-1), jnp.sum(readout * readout, axis=-1)])
        for level_id in range(levels):
            head_stats = head_stats + partner_2(head_stats, "tp", level_id)
        mean_v = head_stats[0][..., None] / DK
        square = head_stats[1][..., None] / DK
        grouped = ((readout - mean_v) * lax.rsqrt(square - mean_v * mean_v + group_eps)).reshape(
            row_total, columns
        )
        grouped = grouped * head_gain[layer_id].astype(jnp.float32)
        gated_rows = (jax.nn.silu(gate_rows.astype(jnp.float32)) * grouped).astype(jnp.bfloat16)
        out_weight = w_out[layer_id]
        term_rows = jnp.dot(
            lax.all_gather(gated_rows, "dp", axis=0, tiled=True),
            out_weight,
            preferred_element_type=jnp.float32,
        )
        branch = summed_on_arrival(term_rows, "tp", 0)
        hidden_x, updated = (
            (x_float + branch).astype(jnp.bfloat16),
            updated.reshape(row_total, columns, DK),
        )
        outputs.append(updated)
    return (hidden_x, jnp.stack(outputs))


def solution(mesh):
    placed = (
        P("tp", "dp"),
        P("dp"),
        P(None, "dp", "tp", None),
        P(None, "dp"),
        P(None, "dp", "tp"),
        P(None, "dp", "tp"),
        P(None, "dp", "tp"),
        P(None, "dp", "tp"),
        P(None, "tp"),
        P(None, "tp", "dp"),
    )
    return jax.shard_map(
        body,
        mesh=mesh,
        in_specs=placed,
        out_specs=(P("tp", "dp"), P(None, "dp", "tp", None)),
        check_vma=False,
    )
```

profile of v0, /device:TPU:1, one launch (start us, length us, event | category | flops | bytes accessed | tf_op | source)
XLA Modules:
  0.0 213.2 jit_solution(16607431848401682273)
XLA Ops:
  0.6 1.4 broadcast_in_dim.4
  2.0 24.1 %all-to-all-start = ((bf16[64,4,256]{2,1,0:T(4,128)(2,1)}), bf16[64,4,256]{2,1,0:T(4,128)(2,1)S(1)}, u32[]{:S(2)}, u32[]{:S(2)}) async-start(bf16[64,4,256]{2,1,0:T(4,128)(2,1)} %broadcast_in_dim.4), calls=%async_computation | async-start | bytes 262144 | tf_op jit(solution)/shard_map/all_to_all | solution.py:27
  26.1 0.7 copy-done.2
  26.9 0.8 copy-done.3
  27.6 0.8 copy-done.4
  28.9 0.6 copy-done.7
  29.4 8.2 %all-to-all-done = bf16[64,4,256]{2,1,0:T(4,128)(2,1)S(1)} async-done(((bf16[64,4,256]{2,1,0:T(4,128)(2,1)}), bf16[64,4,256]{2,1,0:T(4,128)(2,1)S(1)}, u32[]{:S(2)}, u32[]{:S(2)}) %all-to-all-start) | async-done | bytes 131104 | tf_op jit(solution)/shard_map/all_to_all | solution.py:27
  37.6 0.1 multiply_reduce_fusion.1
  37.9 0.3 fusion.4
  38.2 20.4 %all_to_all.30 = f32[16,16,129]{2,1,0:T(8,128)S(1)} all-to-all(f32[16,16,129]{2,1,0:T(8,128)S(1)} %pad_maximum_fusion.1), channel_id=1, replica_groups=mesh['tp'=64,'dp'=16] {'dp'}, dimensions={0} | all-to-all | bytes 264192 | tf_op jit(solution)/shard_map/all_to_all | solution.py:49
  58.9 2.4 %collective-permute-start = (bf16[2,16,32]{2,1,0:T(8,128)(2,1)S(1)}, bf16[2,16,32]{2,1,0:T(8,128)(2,1)S(1)}, u32[]{:S(2)}, u32[]{:S(2)}) collective-permute-start(bf16[2,16,32]{2,1,0:T(8,128)(2,1)S(1)} %pad_maximum_fusion.3), channel_id=1, source_target_pairs={{0,16},{16,0},{32,48},{48,32},{64,80},{80,64},{96,112},{112,96},{1... | collective-permute-start | bytes 6152 | tf_op jit(solution)/shard_map/ppermute | solution.py:22
  61.3 2.0 collective-permute-done
  63.4 2.5 %collective-permute-start.1 = (bf16[2,16,64]{2,1,0:T(8,128)(2,1)S(1)}, bf16[2,16,64]{2,1,0:T(8,128)(2,1)S(1)}, u32[]{:S(2)}, u32[]{:S(2)}) collective-permute-start(bf16[2,16,64]{2,1,0:T(8,128)(2,1)S(1)} %maximum_select_fusion), channel_id=1, source_target_pairs={{0,32},{16,48},{32,0},{48,16},{64,96},{80,112},{96,64},{112,80},{1... | collective-permute-start | bytes 12296 | tf_op jit(solution)/shard_map/ppermute | solution.py:22
  66.0 0.6 copy-done.9
  66.7 2.0 collective-permute-done.1
  69.1 0.2 fusion.1
  69.5 2.4 %collective-permute-start.2 = (f32[2,16,1]{1,2,0:T(1,128)S(1)}, f32[2,16,1]{1,2,0:T(1,128)S(1)}, u32[]{:S(2)}, u32[]{:S(2)}) collective-permute-start(f32[2,16,1]{1,2,0:T(1,128)S(1)} %pad_maximum_fusion.7), channel_id=1, source_target_pairs={{0,16},{16,0},{32,48},{48,32},{64,80},{80,64},{96,112},{112,96},{1... | collective-permute-start | bytes 392 | tf_op jit(solution)/shard_map/ppermute | solution.py:22
  71.8 1.9 collective-permute-done.2
  73.8 2.5 %collective-permute-start.3 = (f32[2,16,1]{1,2,0:T(1,128)S(1)}, f32[2,16,1]{1,2,0:T(1,128)S(1)}, u32[]{:S(2)}, u32[]{:S(2)}) collective-permute-start(f32[2,16,1]{1,2,0:T(1,128)S(1)} %fusion.93), channel_id=1, source_target_pairs={{0,32},{16,48},{32,0},{48,16},{64,96},{80,112},{96,64},{112,80},{1... | collective-permute-start | bytes 392 | tf_op jit(solution)/shard_map/ppermute | solution.py:22
  76.3 2.7 %collective-permute-done.3 = f32[2,16,1]{1,2,0:T(1,128)S(1)} collective-permute-done((f32[2,16,1]{1,2,0:T(1,128)S(1)}, f32[2,16,1]{1,2,0:T(1,128)S(1)}, u32[]{:S(2)}, u32[]{:S(2)}) %collective-permute-start.3) | collective-permute-done | bytes 160 | tf_op jit(solution)/shard_map/ppermute | solution.py:22
  79.1 18.8 %all_gather.6 = bf16[256,32]{1,0:T(8,128)(2,1)S(1)} all-gather(bf16[16,32]{1,0:T(8,128)(2,1)S(1)} %fusion.79), channel_id=1, replica_groups=mesh['tp'=64,'dp'=16] {'dp'}, dimensions={0}, use_global_device_ids=true | all-gather | bytes 17408 | tf_op jit(solution)/shard_map/all_gather | solution.py:147
  97.9 0.2 fusion.28
  98.0 0.2 copy.54
  98.2 17.3 %all_to_all.31 = f32[64,4,256]{2,1,0:T(4,128)S(1)} all-to-all(f32[64,4,256]{2,1,0:T(4,128)S(1)} %copy.54), channel_id=1, replica_groups=mesh['tp'=64,'dp'=16] {'tp'}, dimensions={0} | all-to-all | bytes 524288 | tf_op jit(solution)/shard_map/all_to_all | solution.py:49
  115.6 0.6 copy-done.6
  116.2 0.7 broadcast_in_dim.5
  116.9 5.2 %all-to-all-start.3 = ((bf16[64,4,256]{2,1,0:T(4,128)(2,1)}), bf16[64,4,256]{2,1,0:T(4,128)(2,1)S(1)}, u32[]{:S(2)}, u32[]{:S(2)}) async-start(bf16[64,4,256]{2,1,0:T(4,128)(2,1)} %broadcast_in_dim.5), calls=%async_computation.3 | async-start | bytes 262144 | tf_op jit(solution)/shard_map/all_to_all | solution.py:27
  122.6 11.1 %all-to-all-done.3 = bf16[64,4,256]{2,1,0:T(4,128)(2,1)S(1)} async-done(((bf16[64,4,256]{2,1,0:T(4,128)(2,1)}), bf16[64,4,256]{2,1,0:T(4,128)(2,1)S(1)}, u32[]{:S(2)}, u32[]{:S(2)}) %all-to-all-start.3) | async-done | bytes 131104 | tf_op jit(solution)/shard_map/all_to_all | solution.py:27
  133.6 0.1 multiply_reduce_fusion
  133.9 0.3 fusion.5
  134.2 19.9 %all_to_all.32 = f32[16,16,129]{2,1,0:T(8,128)S(1)} all-to-all(f32[16,16,129]{2,1,0:T(8,128)S(1)} %pad_maximum_fusion.2), channel_id=1, replica_groups=mesh['tp'=64,'dp'=16] {'dp'}, dimensions={0} | all-to-all | bytes 264192 | tf_op jit(solution)/shard_map/all_to_all | solution.py:49
  154.4 2.4 %collective-permute-start.4 = (bf16[2,16,32]{2,1,0:T(8,128)(2,1)S(1)}, bf16[2,16,32]{2,1,0:T(8,128)(2,1)S(1)}, u32[]{:S(2)}, u32[]{:S(2)}) collective-permute-start(bf16[2,16,32]{2,1,0:T(8,128)(2,1)S(1)} %pad_maximum_fusion.5), channel_id=1, source_target_pairs={{0,16},{16,0},{32,48},{48,32},{64,80},{80,64},{96,112},{112,96},{1... | collective-permute-start | bytes 6152 | tf_op jit(solution)/shard_map/ppermute | solution.py:22
  156.9 2.0 collective-permute-done.4
  158.9 2.5 %collective-permute-start.5 = (bf16[2,16,64]{2,1,0:T(8,128)(2,1)S(1)}, bf16[2,16,64]{2,1,0:T(8,128)(2,1)S(1)}, u32[]{:S(2)}, u32[]{:S(2)}) collective-permute-start(bf16[2,16,64]{2,1,0:T(8,128)(2,1)S(1)} %maximum_select_fusion.2), channel_id=1, source_target_pairs={{0,32},{16,48},{32,0},{48,16},{64,96},{80,112},{96,64},{112,80},{1... | collective-permute-start | bytes 12296 | tf_op jit(solution)/shard_map/ppermute | solution.py:22
  161.4 2.8 %collective-permute-done.5 = bf16[2,16,64]{2,1,0:T(8,128)(2,1)S(1)} collective-permute-done((bf16[2,16,64]{2,1,0:T(8,128)(2,1)S(1)}, bf16[2,16,64]{2,1,0:T(8,128)(2,1)S(1)}, u32[]{:S(2)}, u32[]{:S(2)}) %collective-permute-start.5) | collective-permute-done | bytes 4128 | tf_op jit(solution)/shard_map/ppermute | solution.py:22
  164.6 0.2 fusion.3
  164.9 2.4 %collective-permute-start.6 = (f32[2,16,1]{1,2,0:T(1,128)S(1)}, f32[2,16,1]{1,2,0:T(1,128)S(1)}, u32[]{:S(2)}, u32[]{:S(2)}) collective-permute-start(f32[2,16,1]{1,2,0:T(1,128)S(1)} %pad_maximum_fusion.8), channel_id=1, source_target_pairs={{0,16},{16,0},{32,48},{48,32},{64,80},{80,64},{96,112},{112,96},{1... | collective-permute-start | bytes 392 | tf_op jit(solution)/shard_map/ppermute | solution.py:22
  167.4 1.9 collective-permute-done.6
  169.3 2.5 %collective-permute-start.7 = (f32[2,16,1]{1,2,0:T(1,128)S(1)}, f32[2,16,1]{1,2,0:T(1,128)S(1)}, u32[]{:S(2)}, u32[]{:S(2)}) collective-permute-start(f32[2,16,1]{1,2,0:T(1,128)S(1)} %fusion.92), channel_id=1, source_target_pairs={{0,32},{16,48},{32,0},{48,16},{64,96},{80,112},{96,64},{112,80},{1... | collective-permute-start | bytes 392 | tf_op jit(solution)/shard_map/ppermute | solution.py:22
  171.8 2.7 %collective-permute-done.7 = f32[2,16,1]{1,2,0:T(1,128)S(1)} collective-permute-done((f32[2,16,1]{1,2,0:T(1,128)S(1)}, f32[2,16,1]{1,2,0:T(1,128)S(1)}, u32[]{:S(2)}, u32[]{:S(2)}) %collective-permute-start.7) | collective-permute-done | bytes 160 | tf_op jit(solution)/shard_map/ppermute | solution.py:22
  174.6 18.8 %all_gather.7 = bf16[256,32]{1,0:T(8,128)(2,1)S(1)} all-gather(bf16[16,32]{1,0:T(8,128)(2,1)S(1)} %fusion.78), channel_id=1, replica_groups=mesh['tp'=64,'dp'=16] {'dp'}, dimensions={0}, use_global_device_ids=true | all-gather | bytes 17408 | tf_op jit(solution)/shard_map/all_gather | solution.py:147
  193.4 0.1 fusion.26
  193.5 0.9 copy.61
  194.4 4.6 %all-to-all-start.5 = ((f32[64,4,256]{2,1,0:T(4,128)}), f32[64,4,256]{2,1,0:T(4,128)S(1)}, u32[]{:S(2)}, u32[]{:S(2)}) async-start(f32[64,4,256]{2,1,0:T(4,128)} %copy.61), calls=%async_computation.5 | async-start | bytes 524288 | tf_op jit(solution)/shard_map/all_to_all | solution.py:49
  199.0 0.2 fusion
  199.2 0.8 pad_maximum_fusion
  200.0 12.5 %all-to-all-done.5 = f32[64,4,256]{2,1,0:T(4,128)S(1)} async-done(((f32[64,4,256]{2,1,0:T(4,128)}), f32[64,4,256]{2,1,0:T(4,128)S(1)}, u32[]{:S(2)}, u32[]{:S(2)}) %all-to-all-start.5) | async-done | bytes 262176 | tf_op jit(solution)/shard_map/all_to_all | solution.py:49
  212.6 0.6 add_convert_fusion
  (75 shorter events, 3.4 us)
Async XLA Ops:
  2.0 24.1 %copy-start.1 = (bf16[2,256,32]{1,2,0:T(8,128)(2,1)S(1)}, bf16[2,256,32]{1,2,0:T(8,128)(2,1)}, u32[]{:S(2)}) copy-start(bf16[2,256,32]{1,2,0:T(8,128)(2,1)} %param.17) | copy-start | bytes 98308
  2.0 35.6 %all-to-all-start = ((bf16[64,4,256]{2,1,0:T(4,128)(2,1)}), bf16[64,4,256]{2,1,0:T(4,128)(2,1)S(1)}, u32[]{:S(2)}, u32[]{:S(2)}) async-start(bf16[64,4,256]{2,1,0:T(4,128)(2,1)} %broadcast_in_dim.4), calls=%async_computation | async-start | bytes 262144 | tf_op jit(solution)/shard_map/all_to_all | solution.py:27
  26.1 0.8 copy-start.2
  26.9 0.8 copy-start.3
  27.6 0.8 copy-start.4
  28.7 0.7 copy-start.7
  38.2 30.9 %copy-start = (f32[2,16,32,128]{3,2,1,0:T(8,128)S(1)}, f32[2,16,32,128]{3,2,1,0:T(8,128)}, u32[]{:S(2)}) copy-start(f32[2,16,32,128]{3,2,1,0:T(8,128)} %param.12) | copy-start | bytes 1572868
  58.9 4.4 %collective-permute-start = (bf16[2,16,32]{2,1,0:T(8,128)(2,1)S(1)}, bf16[2,16,32]{2,1,0:T(8,128)(2,1)S(1)}, u32[]{:S(2)}, u32[]{:S(2)}) collective-permute-start(bf16[2,16,32]{2,1,0:T(8,128)(2,1)S(1)} %pad_maximum_fusion.3), channel_id=1, source_target_pairs={{0,16},{16,0},{32,48},{48,32},{64,80},{80,64},{96,112},{112,96},{1... | collective-permute-start | bytes 6152 | tf_op jit(solution)/shard_map/ppermute | solution.py:22
  63.4 5.3 %collective-permute-start.1 = (bf16[2,16,64]{2,1,0:T(8,128)(2,1)S(1)}, bf16[2,16,64]{2,1,0:T(8,128)(2,1)S(1)}, u32[]{:S(2)}, u32[]{:S(2)}) collective-permute-start(bf16[2,16,64]{2,1,0:T(8,128)(2,1)S(1)} %maximum_select_fusion), channel_id=1, source_target_pairs={{0,32},{16,48},{32,0},{48,16},{64,96},{80,112},{96,64},{112,80},{1... | collective-permute-start | bytes 12296 | tf_op jit(solution)/shard_map/ppermute | solution.py:22
  66.0 0.7 copy-start.9
  69.5 6.8 %copy-start.8 = (bf16[2,32]{1,0:T(2,128)(2,1)S(1)}, bf16[2,32]{1,0:T(2,128)(2,1)}, u32[]{:S(2)}) copy-start(bf16[2,32]{1,0:T(2,128)(2,1)} %param.18) | copy-start | bytes 388
  69.5 4.3 %collective-permute-start.2 = (f32[2,16,1]{1,2,0:T(1,128)S(1)}, f32[2,16,1]{1,2,0:T(1,128)S(1)}, u32[]{:S(2)}, u32[]{:S(2)}) collective-permute-start(f32[2,16,1]{1,2,0:T(1,128)S(1)} %pad_maximum_fusion.7), channel_id=1, source_target_pairs={{0,16},{16,0},{32,48},{48,32},{64,80},{80,64},{96,112},{112,96},{1... | collective-permute-start | bytes 392 | tf_op jit(solution)/shard_map/ppermute | solution.py:22
  73.8 5.2 %collective-permute-start.3 = (f32[2,16,1]{1,2,0:T(1,128)S(1)}, f32[2,16,1]{1,2,0:T(1,128)S(1)}, u32[]{:S(2)}, u32[]{:S(2)}) collective-permute-start(f32[2,16,1]{1,2,0:T(1,128)S(1)} %fusion.93), channel_id=1, source_target_pairs={{0,32},{16,48},{32,0},{48,16},{64,96},{80,112},{96,64},{112,80},{1... | collective-permute-start | bytes 392 | tf_op jit(solution)/shard_map/ppermute | solution.py:22
  79.1 18.8 %copy-start.5 = (bf16[2,32,256]{2,1,0:T(8,128)(2,1)S(1)}, bf16[2,32,256]{2,1,0:T(8,128)(2,1)}, u32[]{:S(2)}) copy-start(bf16[2,32,256]{2,1,0:T(8,128)(2,1)} %param.19) | copy-start | bytes 98308
  115.5 0.7 copy-start.6
  116.9 16.7 %all-to-all-start.3 = ((bf16[64,4,256]{2,1,0:T(4,128)(2,1)}), bf16[64,4,256]{2,1,0:T(4,128)(2,1)S(1)}, u32[]{:S(2)}, u32[]{:S(2)}) async-start(bf16[64,4,256]{2,1,0:T(4,128)(2,1)} %broadcast_in_dim.5), calls=%async_computation.3 | async-start | bytes 262144 | tf_op jit(solution)/shard_map/all_to_all | solution.py:27
  154.4 4.4 %collective-permute-start.4 = (bf16[2,16,32]{2,1,0:T(8,128)(2,1)S(1)}, bf16[2,16,32]{2,1,0:T(8,128)(2,1)S(1)}, u32[]{:S(2)}, u32[]{:S(2)}) collective-permute-start(bf16[2,16,32]{2,1,0:T(8,128)(2,1)S(1)} %pad_maximum_fusion.5), channel_id=1, source_target_pairs={{0,16},{16,0},{32,48},{48,32},{64,80},{80,64},{96,112},{112,96},{1... | collective-permute-start | bytes 6152 | tf_op jit(solution)/shard_map/ppermute | solution.py:22
  158.9 5.3 %collective-permute-start.5 = (bf16[2,16,64]{2,1,0:T(8,128)(2,1)S(1)}, bf16[2,16,64]{2,1,0:T(8,128)(2,1)S(1)}, u32[]{:S(2)}, u32[]{:S(2)}) collective-permute-start(bf16[2,16,64]{2,1,0:T(8,128)(2,1)S(1)} %maximum_select_fusion.2), channel_id=1, source_target_pairs={{0,32},{16,48},{32,0},{48,16},{64,96},{80,112},{96,64},{112,80},{1... | collective-permute-start | bytes 12296 | tf_op jit(solution)/shard_map/ppermute | solution.py:22
  164.9 4.3 %collective-permute-start.6 = (f32[2,16,1]{1,2,0:T(1,128)S(1)}, f32[2,16,1]{1,2,0:T(1,128)S(1)}, u32[]{:S(2)}, u32[]{:S(2)}) collective-permute-start(f32[2,16,1]{1,2,0:T(1,128)S(1)} %pad_maximum_fusion.8), channel_id=1, source_target_pairs={{0,16},{16,0},{32,48},{48,32},{64,80},{80,64},{96,112},{112,96},{1... | collective-permute-start | bytes 392 | tf_op jit(solution)/shard_map/ppermute | solution.py:22
  169.3 5.2 %collective-permute-start.7 = (f32[2,16,1]{1,2,0:T(1,128)S(1)}, f32[2,16,1]{1,2,0:T(1,128)S(1)}, u32[]{:S(2)}, u32[]{:S(2)}) collective-permute-start(f32[2,16,1]{1,2,0:T(1,128)S(1)} %fusion.92), channel_id=1, source_target_pairs={{0,32},{16,48},{32,0},{48,16},{64,96},{80,112},{96,64},{112,80},{1... | collective-permute-start | bytes 392 | tf_op jit(solution)/shard_map/ppermute | solution.py:22
  194.4 18.1 %all-to-all-start.5 = ((f32[64,4,256]{2,1,0:T(4,128)}), f32[64,4,256]{2,1,0:T(4,128)S(1)}, u32[]{:S(2)}, u32[]{:S(2)}) async-start(f32[64,4,256]{2,1,0:T(4,128)} %copy.61), calls=%async_computation.5 | async-start | bytes 524288 | tf_op jit(solution)/shard_map/all_to_all | solution.py:49
where the time goes:
time: 215 us; the launch traced here: 213 us
  blocking collectives  95.2 us (44%)
  starting transfers between devices  53.3 us (25%)
  waiting for transfers between devices  49.8 us (23%)
  local copies, waits for them, and re-layouts  8.34 us (4%)
  other arithmetic  4.11 us (2%)
    all_to_all x3, blocking collectives, summed_on_arrival(): lax.all_to_all(cut_along(shard, dim, count), axis, 0, 0, tiled=True)  57.6 us
    all_gather x2, blocking collectives, body(): lax.all_gather(gated_rows, 'dp', axis=0, tiled=True)  37.5 us
    all_to_all x2, starting transfers between devices, sent_to_all(): return lax.all_to_all(copies, axis, split_axis=0, concat_axis=0, tiled=True)  29.2 us
    ppermute x8, starting transfers between devices, partner_2(): return lax.ppermute(value, axis, pairs)  19.5 us
    all_to_all x2, waiting for transfers between devices, sent_to_all(): return lax.all_to_all(copies, axis, split_axis=0, concat_axis=0, tiled=True)  19.2 us
    ppermute x8, waiting for transfers between devices, partner_2(): return lax.ppermute(value, axis, pairs)  18 us
    all_to_all x1, waiting for transfers between devices, summed_on_arrival(): lax.all_to_all(cut_along(shard, dim, count), axis, 0, 0, tiled=True)  12.5 us
    unnamed x28, local copies, waits for them, and re-layouts  5.01 us
  transfers between devices with their start and end apart: 11, of which 11 were waited for; matrix products, arithmetic and copies ran while one was open for 1% of the time, Pallas kernels for 0%

commit v1 on v0

v1 whole, which is shorter than its diff:
```python
import functools

import jax
import jax.numpy as jnp
from jax import lax
from jax.experimental import pallas as pl
from jax.experimental.pallas import tpu as pltpu
from jax.sharding import PartitionSpec as P

D = 4096
HEADS = 16
DK = 128
LAYERS = 2
TP = 64
DP = 16
ROWS = 4
FEATS = 256
COLS = 32
SEQ = 16
GROUP = 4

norm_eps = 1e-06
group_eps = 1e-05
rotary_base = 10000.0
MESH = pl.DeviceIdType.MESH
f32 = jnp.float32
bf16 = jnp.bfloat16


def far_first(a):
    return lax.rem(4 + (2 * lax.rem(a, 2) - 1) * lax.div(a + 1, 2) + 8, 8)


def kernel(
    tok, lens, states, ngain, wq, wk, wv, wg, hgain, wout,
    out, st_out,
    len_s, xo, xg, nrm, wp, wo, ng, hg, st,
    p2s, p2r, sqs, sqr, pj, sts, str_, g5s, g5r, of, p6s, p6r,
    lsem, csem, osem, ss, rs,
):
    tp = lax.axis_index("tp")
    dp = lax.axis_index("dp")
    z, y = lax.div(tp, 8), lax.rem(tp, 8)
    xc, core = lax.div(dp, 2), lax.rem(dp, 2)
    grp, gj = lax.div(tp, GROUP), lax.rem(tp, GROUP)

    def tp_peer(k):
        dz, dy = far_first(lax.div(k, 8)), far_first(lax.rem(k, 8))
        return lax.rem(z + dz, 8) * 8 + lax.rem(y + dy, 8)

    def dp_peer(k):
        dx = far_first(lax.div(k, 2))
        return lax.rem(xc + dx, 8) * 2 + lax.rem(core + 1 - lax.rem(k, 2), 2)

    def group_peer(k):
        return grp * GROUP + lax.rem(gj + k, GROUP)

    loads = [
        pltpu.make_async_copy(tok, xo.at[0], lsem.at[0]),
        pltpu.make_async_copy(lens, len_s, lsem.at[1]),
        pltpu.make_async_copy(states, st, lsem.at[2]),
        pltpu.make_async_copy(ngain, ng, lsem.at[3]),
        pltpu.make_async_copy(wq, wp.at[:, 0:32], lsem.at[4]),
        pltpu.make_async_copy(wk, wp.at[:, 32:64], lsem.at[5]),
        pltpu.make_async_copy(wv, wp.at[:, 64:96], lsem.at[6]),
        pltpu.make_async_copy(wg, wp.at[:, 96:128], lsem.at[7]),
        pltpu.make_async_copy(hgain, hg, lsem.at[8]),
        pltpu.make_async_copy(wout, wo.at[:, 0:32], lsem.at[9]),
    ]
    for c in loads:
        c.start()

    barrier = pltpu.get_barrier_semaphore()

    def greet_tp(k, _):
        pl.semaphore_signal(barrier, inc=1, device_id=(tp_peer(k), dp), device_id_type=MESH)
        return 0

    def greet_dp(k, _):
        pl.semaphore_signal(barrier, inc=1, device_id=(tp, dp_peer(k)), device_id_type=MESH)
        return 0

    lax.fori_loop(0, TP - 1, greet_tp, 0)
    lax.fori_loop(0, DP - 1, greet_dp, 0)

    for c in loads:
        c.wait()
    row = lax.broadcasted_iota(jnp.int32, (SEQ, DK), 0)
    lane = lax.broadcasted_iota(jnp.int32, (SEQ, DK), 1)
    diag = row == lane
    lane32 = lax.broadcasted_iota(jnp.int32, (COLS, DK), 1)
    row32 = lax.broadcasted_iota(jnp.int32, (COLS, COLS), 0)
    col32 = lax.broadcasted_iota(jnp.int32, (COLS, COLS), 1)
    pos = jnp.zeros((SEQ, DK), jnp.int32)
    for s in range(SEQ):
        pos = jnp.where(row == s, len_s[s], pos)
    half = DK // 2
    exponent = lax.rem(lane, half).astype(f32) / half
    inverse = jnp.exp(exponent * (-9.210340371976184))
    angle = pos.astype(f32) * inverse
    cosine = jnp.cos(angle)
    sine = jnp.sin(angle)
    sine = jnp.where(lane < half, -sine, sine)
    wo[:, 32:128, :] = jnp.zeros((LAYERS, 96, FEATS), bf16)
    head = (jnp.zeros((COLS, DK), jnp.int32) + grp).astype(f32)
    gamma = 1.0 - jnp.exp2(-1.0 - 9.0 * head / (HEADS - 1))
    hgains = [
        jnp.sum(jnp.where(row32 == col32, hg[l : l + 1, :].astype(f32), 0.0), axis=1, keepdims=True)
        for l in range(LAYERS)
    ]
    pad_rows = jnp.zeros((DK - SEQ, DK), f32)

    pl.semaphore_wait(barrier, TP + DP - 2)

    outs = []
    sends = []

    def send_tp(src_of, dst, sem_id):
        def step(k, _):
            peer = tp_peer(k)
            pltpu.make_async_remote_copy(
                src_ref=src_of(peer), dst_ref=dst, send_sem=ss.at[sem_id], recv_sem=rs.at[sem_id],
                device_id=(peer, dp), device_id_type=MESH,
            ).start()
            return 0

        lax.fori_loop(0, TP - 1, step, 0)

    def send_dp(src_of, dst, sem_id):
        def step(k, _):
            peer = dp_peer(k)
            pltpu.make_async_remote_copy(
                src_ref=src_of(peer), dst_ref=dst, send_sem=ss.at[sem_id], recv_sem=rs.at[sem_id],
                device_id=(tp, peer), device_id_type=MESH,
            ).start()
            return 0

        lax.fori_loop(0, DP - 1, step, 0)

    def send_group(src, dst, sem_id):
        for k in (3, 2, 1):
            pltpu.make_async_remote_copy(
                src_ref=src, dst_ref=dst, send_sem=ss.at[sem_id], recv_sem=rs.at[sem_id],
                device_id=(group_peer(k), dp), device_id_type=MESH,
            ).start()

    def wait_bytes(ref, sem):
        pltpu.make_async_copy(ref, ref, sem).wait()

    for l in range(LAYERS):
        b = 7 * l
        send_tp(lambda peer: xo.at[l], xg.at[l, tp], b)
        xg[l, tp] = xo[l]
        wait_bytes(xg.at[l, pl.ds(0, TP - 1)], rs.at[b])
        sends.append((xg.at[l, pl.ds(0, TP - 1)], b))
        gain = ng[l : l + 1, :].astype(f32)
        for d in range(DP):
            xf = jnp.concatenate([xg[l, 4 * d + j].astype(f32) for j in range(4)], axis=0)
            squares = jnp.sum(xf * xf, axis=1, keepdims=True)
            sqs[l, d] = jnp.sum(jnp.where(diag, squares, 0.0), axis=0, keepdims=True)
            nrm[pl.ds(SEQ * d, SEQ), :] = (xf * gain).astype(bf16)
        part = lax.dot_general(
            nrm[...], wp[l], (((1,), (1,)), ((), ())), preferred_element_type=f32
        )
        p2s[l] = part.astype(bf16).reshape(DP, SEQ, DK)
        send_dp(lambda peer: p2s.at[l, peer], p2r.at[l, dp], b + 1)
        send_dp(lambda peer: sqs.at[l, peer], sqr.at[l, dp], b + 2)
        p2r[l, dp] = p2s[l, dp]
        sqr[l, dp] = sqs[l, dp]
        wait_bytes(p2r.at[l, pl.ds(0, DP - 1)], rs.at[b + 1])
        wait_bytes(sqr.at[l, pl.ds(0, DP - 1)], rs.at[b + 2])
        sends.append((p2r.at[l, pl.ds(0, DP - 1)], b + 1))
        sends.append((sqr.at[l, pl.ds(0, DP - 1)], b + 2))
        total = jnp.sum(p2r[l].astype(f32), axis=0)
        squares = jnp.sum(sqr[l], axis=0)
        squares = jnp.sum(jnp.where(diag, squares, 0.0), axis=1, keepdims=True)
        row_scale = lax.rsqrt(squares / D + norm_eps)
        proj = (total * row_scale).astype(bf16)
        pj[l, gj] = proj
        send_group(pj.at[l, gj], pj.at[l, gj], b + 3)
        proj_f = proj.astype(f32)
        proj_t = jnp.transpose(jnp.concatenate([proj_f, pad_rows], axis=0))
        values_t = proj_t[64:96, :]
        gate_t = proj_t[96:128, :]
        silu_t = gate_t / (1.0 + jnp.exp(-gate_t))
        wait_bytes(pj.at[l, pl.ds(0, GROUP - 1)], rs.at[b + 3])
        sends.append((pj.at[l, pl.ds(0, GROUP - 1)], b + 3))
        query = jnp.zeros((SEQ, DK), f32)
        key = jnp.zeros((SEQ, DK), f32)
        for j in range(GROUP):
            piece = pj[l, j].astype(f32)
            here = lax.div(lane, 32) == j
            query = jnp.where(here, pltpu.roll(piece, 32 * j, 1) if j else piece, query)
            shift = (32 * j - 32) % DK
            key = jnp.where(here, pltpu.roll(piece, shift, 1) if shift else piece, key)
        rq = query * cosine + pltpu.roll(query, half, 1) * sine
        rk = (key * cosine + pltpu.roll(key, half, 1) * sine) * DK ** (-0.5)
        read = jnp.zeros((COLS, DK), f32)
        for s in range(SEQ):
            new = gamma * st[l, s] + values_t[:, s : s + 1] * rk[s : s + 1, :]
            st[l, s] = new
            r = jnp.sum(new * rq[s : s + 1, :], axis=1, keepdims=True)
            read = jnp.where(lane32 == s, r, read)
        sts[l, 0:1] = jnp.sum(read, axis=0, keepdims=True)
        sts[l, 1:2] = jnp.sum(read * read, axis=0, keepdims=True)
        send_group(sts.at[l], str_.at[l, gj], b + 4)
        copy = pltpu.make_async_copy(st.at[l], st_out.at[l], osem.at[l])
        copy.start()
        outs.append(copy)
        str_[l, gj] = sts[l]
        wait_bytes(str_.at[l, pl.ds(0, GROUP - 1)], rs.at[b + 4])
        sends.append((str_.at[l, pl.ds(0, GROUP - 1)], b + 4))
        both = (str_[l, 0] + str_[l, 1]) + (str_[l, 2] + str_[l, 3])
        mean_v = both[0:1, :] / DK
        square = both[1:2, :] / DK
        grouped = (read - mean_v) * lax.rsqrt(square - mean_v * mean_v + group_eps) * hgains[l]
        gated = silu_t * grouped
        gated = jnp.concatenate([gated, jnp.zeros((DK - COLS, DK), f32)], axis=0)
        gated = jnp.transpose(gated)[0:SEQ, :].astype(bf16)
        g5s[l] = gated
        send_dp(lambda peer: g5s.at[l], g5r.at[l, dp], b + 5)
        g5r[l, dp] = gated
        wait_bytes(g5r.at[l, pl.ds(0, DP - 1)], rs.at[b + 5])
        sends.append((g5r.at[l, pl.ds(0, DP - 1)], b + 5))
        of[...] = jnp.dot(
            g5r[l].reshape(DP * SEQ, DK), wo[l], preferred_element_type=f32
        )
        for t in range(TP):
            p6s[l, t] = of[pl.ds(ROWS * t, ROWS), :].astype(bf16)
        send_tp(lambda peer: p6s.at[l, peer], p6r.at[l, tp], b + 6)
        p6r[l, tp] = p6s[l, tp]
        wait_bytes(p6r.at[l, pl.ds(0, TP - 1)], rs.at[b + 6])
        sends.append((p6r.at[l, pl.ds(0, TP - 1)], b + 6))
        branch = jnp.sum(p6r[l].astype(f32), axis=0)
        x_new = (xo[l].astype(f32) + branch).astype(bf16)
        if l + 1 < LAYERS:
            xo[l + 1] = x_new
        else:
            out[...] = x_new

    for ref, sem_id in sends:
        wait_bytes(ref, ss.at[sem_id])
    for c in outs:
        c.wait()


def body(tokens, lengths, states, norm_gain, w_query, w_key, w_value, w_gate, head_gain, w_out):
    flip = lambda w: jnp.transpose(w, (0, 2, 1))
    hbm = pl.BlockSpec(memory_space=pl.ANY)
    vmem = pltpu.VMEM
    return pl.pallas_call(
        kernel,
        out_shape=(
            jax.ShapeDtypeStruct((ROWS, FEATS), bf16),
            jax.ShapeDtypeStruct(states.shape, f32),
        ),
        in_specs=[hbm] * 10,
        out_specs=(pl.BlockSpec(memory_space=pltpu.VMEM), hbm),
        scratch_shapes=[
            pltpu.SMEM((SEQ,), jnp.int32),
            vmem((LAYERS, ROWS, FEATS), bf16),
            vmem((LAYERS, TP, ROWS, FEATS), bf16),
            vmem((TP * ROWS, FEATS), bf16),
            vmem((LAYERS, DK, FEATS), bf16),
            vmem((LAYERS, DK, FEATS), bf16),
            vmem((LAYERS, FEATS), bf16),
            vmem((LAYERS, COLS), bf16),
            vmem((LAYERS, SEQ, COLS, DK), f32),
            vmem((LAYERS, DP, SEQ, DK), bf16),
            vmem((LAYERS, DP, SEQ, DK), bf16),
            vmem((LAYERS, DP, 1, DK), f32),
            vmem((LAYERS, DP, 1, DK), f32),
            vmem((LAYERS, GROUP, SEQ, DK), bf16),
            vmem((LAYERS, 2, DK), f32),
            vmem((LAYERS, GROUP, 2, DK), f32),
            vmem((LAYERS, SEQ, DK), bf16),
            vmem((LAYERS, DP, SEQ, DK), bf16),
            vmem((DP * SEQ, FEATS), f32),
            vmem((LAYERS, TP, ROWS, FEATS), bf16),
            vmem((LAYERS, TP, ROWS, FEATS), bf16),
            pltpu.SemaphoreType.DMA((10,)),
            pltpu.SemaphoreType.DMA((1,)),
            pltpu.SemaphoreType.DMA((LAYERS,)),
            pltpu.SemaphoreType.DMA((7 * LAYERS,)),
            pltpu.SemaphoreType.DMA((7 * LAYERS,)),
        ],
        compiler_params=pltpu.CompilerParams(collective_id=0, has_side_effects=True),
        name="retention_step",
    )(
        tokens, lengths, states, norm_gain,
        flip(w_query), flip(w_key), flip(w_value), flip(w_gate), head_gain, w_out,
    )


def solution(mesh):
    placed = (
        P("tp", "dp"),
        P("dp"),
        P(None, "dp", "tp", None),
        P(None, "dp"),
        P(None, "dp", "tp"),
        P(None, "dp", "tp"),
        P(None, "dp", "tp"),
        P(None, "dp", "tp"),
        P(None, "tp"),
        P(None, "tp", "dp"),
    )
    return jax.shard_map(
        body,
        mesh=mesh,
        in_specs=placed,
        out_specs=(P("tp", "dp"), P(None, "dp", "tp", None)),
        check_vma=False,
    )
```

time: 215 us -> 95.2 us (0.44)
  blocking collectives: 95.2 us -> 0 us
  Pallas kernels: 0 us -> 91.2 us
  starting transfers between devices: 53.3 us -> 0 us
  waiting for transfers between devices: 49.8 us -> 0 us
  local copies, waits for them, and re-layouts: 8.34 us -> 3.11 us
  other arithmetic: 4.11 us -> 0 us
    pallas_call x0 -> x1, Pallas kernels: none -> 91.2 us  [body(): pl.pallas_call(kernel, out_shape=(jax.ShapeDtypeStruct((ROWS, FEATS), bf1...]
    all_to_all x3 -> x0, blocking collectives: 57.6 us -> none  [summed_on_arrival(): lax.all_to_all(cut_along(shard, dim, count), axis, 0, 0, tiled=True)]
    all_gather x2 -> x0, blocking collectives: 37.5 us -> none  [body(): lax.all_gather(gated_rows, 'dp', axis=0, tiled=True)]
    all_to_all x3 -> x0, starting transfers between devices: 33.8 us -> none  [the longest x2 29.2 us: sent_to_all(): return lax.all_to_all(copies, axis, split_axis=0, concat_axis=0, tiled=True)]
    all_to_all x3 -> x0, waiting for transfers between devices: 31.7 us -> none  [the longest x2 19.2 us: sent_to_all(): return lax.all_to_all(copies, axis, split_axis=0, concat_axis=0, tiled=True)]
    ppermute x8 -> x0, starting transfers between devices: 19.5 us -> none  [partner_2(): return lax.ppermute(value, axis, pairs)]
    ppermute x8 -> x0, waiting for transfers between devices: 18 us -> none  [partner_2(): return lax.ppermute(value, axis, pairs)]
    unnamed x28 -> x4, local copies, waits for them, and re-layouts: 5.01 us -> 3.11 us
  transfers between devices with their start and end apart: 11 -> 0, of which waited for: 11 -> 0; matrix products, arithmetic and copies ran while one was open for 1% -> 0% of each run, Pallas kernels for 0% -> 0%
where the time goes in v1:
time: 95.2 us; the launch traced here: 95 us
  Pallas kernels  91.2 us (96%)
  local copies, waits for them, and re-layouts  3.11 us (3%)
    pallas_call x1, Pallas kernels, body(): pl.pallas_call(kernel, out_shape=(jax.ShapeDtypeStruct((ROWS, FEATS), bf1...  91.2 us
    unnamed x4, local copies, waits for them, and re-layouts  3.11 us

profile of v1, /device:TPU:1, one launch (start us, length us, event | category | flops | bytes accessed | tf_op | source)
XLA Modules:
  0.0 95.0 jit_solution(2603368540729136984)
XLA Ops:
  0.6 91.2 %retention_step.1 = (bf16[4,256]{1,0:T(4,128)(2,1)}, f32[2,16,32,128]{3,2,1,0:T(8,128)}) custom-call(bf16[4,256]{1,0:T(4,128)(2,1)} %tok.1, s32[16]{0:T(128)} %lens.1, f32[2,16,32,128]{3,2,1,0:T(8,128)} %states.1, bf16[2,256]{1,0:T(2,128)(2,1)} %ngain.1, bf16[2,32,256]{2,1,0:T(8,128)(2,1)} %bitcast.4, bf16[2,32,256]{2,1,0:T(8,128)(2,1)} %bitcast.5, ...), custom_call_target="tpu_custom_call" | custom-call | tf_op jit(solution)/shard_map/retention_step/pallas_call | solution.py:251
  91.9 0.0 copy-start
  91.9 0.7 copy-done
  92.6 0.6 copy.14
  93.1 1.9 %copy.15 = f32[2,16,32,128]{3,2,1,0:T(8,128)} copy(f32[2,16,32,128]{3,2,1,0:T(8,128)} %get-tuple-element.5) | data formatting | bytes 1048576
Async XLA Ops:
  91.9 0.7 copy-start

commit v2 on v1

v2 whole, which is shorter than its diff:
```python
import jax
import jax.numpy as jnp
from jax import lax
from jax.experimental import pallas as pl
from jax.experimental.pallas import tpu as pltpu
from jax.sharding import PartitionSpec as P

D = 4096
HEADS = 16
DK = 128
LAYERS = 2
TP = 64
DP = 16
RING = 8
ROWS = 4
FEATS = 256
COLS = 32
SEQ = 16
GROUP = 4
FAR = (4, 5, 3, 6, 2, 7, 1, 0)
WIDE = DK + COLS

norm_eps = 1e-06
group_eps = 1e-05
rotary_base = 10000.0
MESH = pl.DeviceIdType.MESH
f32 = jnp.float32
bf16 = jnp.bfloat16


def hops(a):
    return min(a, RING - a)


PLANE = sorted(
    ((dz, dy) for dz in range(RING) for dy in range(RING) if dz or dy),
    key=lambda o: -(hops(o[0]) + hops(o[1])),
)


def kernel(
    tok, lens, states, ngain, wq, wk, wv, wg, hgain, wout,
    out, st,
    len_s, xo, xg, nrm, wp0, wp1, wo0, w1, ng, hg,
    p2s, p2r, sqs, sqr, pj, sts, str_, res_s, res, p6s, p6r, xb, xg1, pfs, pfr,
    lsem, ring_r, ring_l, sib_r, side_s, ss, rs,
):
    tp = lax.axis_index("tp")
    dp = lax.axis_index("dp")
    z, y = lax.div(tp, RING), lax.rem(tp, RING)
    xc, core = lax.div(dp, 2), lax.rem(dp, 2)
    other = 1 - core
    grp, gj = lax.div(tp, GROUP), lax.rem(tp, GROUP)
    z8 = [lax.rem(z + o, RING) * RING for o in range(RING)]
    yo = [lax.rem(y + o, RING) for o in range(RING)]
    xo2 = [lax.rem(xc + o, RING) for o in range(RING)]
    tp_peers = [z8[dz] + yo[dy] for dz, dy in PLANE]
    line = [(o, c) for o in FAR for c in (0, 1) if o or c]
    dp_peers = [xo2[o] * 2 + (other if c else core) for o, c in line]
    group_peers = [grp * GROUP + lax.rem(gj + k, GROUP) for k in (3, 2, 1)]

    loads = [
        pltpu.make_async_copy(tok, xo, lsem.at[0]),
        pltpu.make_async_copy(wout.at[0], wo0.at[core, xc], lsem.at[1]),
        pltpu.make_async_copy(wq.at[1], wp1.at[0:32], lsem.at[2]),
        pltpu.make_async_copy(wk.at[1], wp1.at[32:64], lsem.at[3]),
        pltpu.make_async_copy(wv.at[1], wp1.at[64:96], lsem.at[4]),
        pltpu.make_async_copy(wg.at[1], wp1.at[96:128], lsem.at[5]),
        pltpu.make_async_copy(wout.at[1], w1.at[core, xc, DK:WIDE], lsem.at[6]),
        pltpu.make_async_copy(ngain, ng, lsem.at[7]),
        pltpu.make_async_copy(wq.at[0], wp0.at[0:32], lsem.at[8]),
        pltpu.make_async_copy(wk.at[0], wp0.at[32:64], lsem.at[9]),
        pltpu.make_async_copy(wv.at[0], wp0.at[64:96], lsem.at[10]),
        pltpu.make_async_copy(wg.at[0], wp0.at[96:128], lsem.at[11]),
        pltpu.make_async_copy(lens, len_s, lsem.at[12]),
        pltpu.make_async_copy(hgain, hg, lsem.at[13]),
        pltpu.make_async_copy(states, st, lsem.at[14]),
    ]
    barrier = pltpu.get_barrier_semaphore()
    for peer in tp_peers:
        pl.semaphore_signal(barrier, inc=1, device_id=(peer, dp), device_id_type=MESH)
    for peer in dp_peers:
        pl.semaphore_signal(barrier, inc=1, device_id=(tp, peer), device_id_type=MESH)
    for c in loads:
        c.start()

    for c in loads:
        c.wait()
    row = lax.broadcasted_iota(jnp.int32, (SEQ, DK), 0)
    lane = lax.broadcasted_iota(jnp.int32, (SEQ, DK), 1)
    diag = row == lane
    lane32 = lax.broadcasted_iota(jnp.int32, (COLS, DK), 1)
    row32 = lax.broadcasted_iota(jnp.int32, (COLS, COLS), 0)
    col32 = lax.broadcasted_iota(jnp.int32, (COLS, COLS), 1)
    pos = jnp.zeros((SEQ, DK), jnp.int32)
    for s in range(SEQ):
        pos = jnp.where(row == s, len_s[s], pos)
    half = DK // 2
    exponent = lax.rem(lane, half).astype(f32) / half
    inverse = jnp.exp(exponent * (-9.210340371976184))
    angle = pos.astype(f32) * inverse
    cosine = jnp.cos(angle)
    sine = jnp.sin(angle)
    sine = jnp.where(lane < half, -sine, sine)
    head = (jnp.zeros((COLS, DK), jnp.int32) + grp).astype(f32)
    gamma = 1.0 - jnp.exp2(-1.0 - 9.0 * head / (HEADS - 1))
    hgains = [
        jnp.sum(jnp.where(row32 == col32, hg[l : l + 1, :].astype(f32), 0.0), axis=1, keepdims=True)
        for l in range(LAYERS)
    ]
    pad_rows = jnp.zeros((DK - SEQ, DK), f32)
    w1[core, xc, 0:DK] = (wp1[...].astype(f32) * ng[1:2, :].astype(f32)).astype(bf16)

    pl.semaphore_wait(barrier, TP + DP - 2)

    sends = []

    def push(src, dst, sem_id, peer_tp, peer_dp):
        pltpu.make_async_remote_copy(
            src_ref=src, dst_ref=dst, send_sem=ss.at[sem_id], recv_sem=rs.at[sem_id],
            device_id=(peer_tp, peer_dp), device_id_type=MESH,
        ).start()

    def push_side(src, dst, recv, peer_dp):
        pltpu.make_async_remote_copy(
            src_ref=src, dst_ref=dst, send_sem=side_s, recv_sem=recv,
            device_id=(tp, peer_dp), device_id_type=MESH,
        ).start()

    def send_group(src, dst, sem_id):
        for peer in group_peers:
            push(src, dst, sem_id, peer, dp)

    def wait_bytes(ref, sem):
        pltpu.make_async_copy(ref, ref, sem).wait()

    def landed(ref, sem_id):
        wait_bytes(ref, rs.at[sem_id])
        sends.append((ref, sem_id))

    right, left, sibling = xo2[1] * 2 + core, xo2[7] * 2 + core, xc * 2 + other

    def ring(step):
        came_right, came_left = xo2[(RING - step) % RING], xo2[step]
        if 1 <= step <= 4:
            wait_bytes(w1.at[core, came_right], ring_r.at[step - 1])
        if 1 <= step <= 3:
            wait_bytes(w1.at[core, came_left], ring_l.at[step - 1])
        if step <= 3:
            push_side(w1.at[core, came_right], w1.at[core, came_right], ring_r.at[step], right)
        if step <= 2:
            push_side(w1.at[core, came_left], w1.at[core, came_left], ring_l.at[step], left)
        if step == 4:
            push_side(w1.at[core], w1.at[core], sib_r.at[1], sibling)

    def projected(proj, sem_id, l, meanwhile):
        pj[l, gj] = proj
        send_group(pj.at[l, gj], pj.at[l, gj], sem_id)
        proj_t = jnp.transpose(jnp.concatenate([proj.astype(f32), pad_rows], axis=0))
        values_t = proj_t[64:96, :]
        gate_t = proj_t[96:128, :]
        silu_t = gate_t / (1.0 + jnp.exp(-gate_t))
        meanwhile()
        landed(pj.at[l, pl.ds(0, GROUP - 1)], sem_id)
        query = jnp.zeros((SEQ, DK), f32)
        key = jnp.zeros((SEQ, DK), f32)
        for j in range(GROUP):
            piece = pj[l, j].astype(f32)
            here = lax.div(lane, 32) == j
            query = jnp.where(here, pltpu.roll(piece, 32 * j, 1) if j else piece, query)
            shift = (32 * j - 32) % DK
            key = jnp.where(here, pltpu.roll(piece, shift, 1) if shift else piece, key)
        rq = query * cosine + pltpu.roll(query, half, 1) * sine
        rk = (key * cosine + pltpu.roll(key, half, 1) * sine) * DK ** (-0.5)
        return rq, rk, values_t, silu_t

    def retained(rq, rk, values_t, silu_t, sem_id, l, meanwhile):
        read = jnp.zeros((COLS, DK), f32)
        for s in range(SEQ):
            new = gamma * st[l, s] + values_t[:, s : s + 1] * rk[s : s + 1, :]
            st[l, s] = new
            r = jnp.sum(new * rq[s : s + 1, :], axis=1, keepdims=True)
            read = jnp.where(lane32 == s, r, read)
        sts[l, 0:1] = jnp.sum(read, axis=0, keepdims=True)
        sts[l, 1:2] = jnp.sum(read * read, axis=0, keepdims=True)
        send_group(sts.at[l], str_.at[l, gj], sem_id)
        str_[l, gj] = sts[l]
        meanwhile()
        landed(str_.at[l, pl.ds(0, GROUP - 1)], sem_id)
        both = (str_[l, 0] + str_[l, 1]) + (str_[l, 2] + str_[l, 3])
        mean_v = both[0:1, :] / DK
        square = both[1:2, :] / DK
        grouped = (read - mean_v) * lax.rsqrt(square - mean_v * mean_v + group_eps) * hgains[l]
        gated = jnp.concatenate([silu_t * grouped, jnp.zeros((DK - COLS, DK), f32)], axis=0)
        return jnp.transpose(gated)[0:SEQ, 0:COLS].astype(bf16)

    for peer in tp_peers:
        push(xo, xg.at[tp], 0, peer, dp)
    xg[tp] = xo[...]
    for o in FAR[:7]:
        push_side(wo0.at[core, xc], wo0.at[core, xc], sib_r.at[2], xo2[o] * 2 + core)
    ring(0)
    landed(xg.at[pl.ds(0, TP - 1)], 0)
    gain = ng[0:1, :].astype(f32)
    res_half, res_side = lax.div(tp, 32), lax.rem(tp, 2)
    for d in range(DP):
        xf = jnp.concatenate([xg[4 * d + j].astype(f32) for j in range(4)], axis=0)
        squares = jnp.sum(xf * xf, axis=1, keepdims=True)
        sqs[d] = jnp.sum(jnp.where(diag, squares, 0.0), axis=0, keepdims=True)
        nrm[pl.ds(SEQ * d, SEQ), :] = (xf * gain).astype(bf16)
        part8 = jnp.where(res_half == 1, xf[8:16], xf[0:8])
        res_s[d] = jnp.where(res_side == 1, part8[:, DK:], part8[:, :DK]).astype(bf16)
    part = lax.dot_general(
        nrm[...], wp0[...], (((1,), (1,)), ((), ())), preferred_element_type=f32
    )
    p2s[...] = part.astype(bf16).reshape(DP, SEQ, DK)
    for peer in dp_peers:
        push(p2s.at[peer], p2r.at[dp], 1, tp, peer)
        push(sqs.at[peer], sqr.at[dp], 2, tp, peer)
    p2r[dp] = p2s[dp]
    sqr[dp] = sqs[dp]
    res_owner = lax.rem(lax.div(tp, 2), DP)

    @pl.when(dp == res_owner)
    def _():
        for peer in dp_peers:
            push(res_s.at[peer], res, 3, tp, peer)
        res[...] = res_s[dp]

    landed(p2r.at[pl.ds(0, DP - 1)], 1)
    landed(sqr.at[pl.ds(0, DP - 1)], 2)
    total = jnp.sum(p2r[...].astype(f32), axis=0)
    squares = jnp.sum(sqr[...], axis=0)
    squares = jnp.sum(jnp.where(diag, squares, 0.0), axis=1, keepdims=True)
    proj = (total * lax.rsqrt(squares / D + norm_eps)).astype(bf16)

    def share_first_out():
        wait_bytes(wo0.at[core, pl.ds(0, RING - 1)], sib_r.at[2])
        push_side(wo0.at[core], wo0.at[core], sib_r.at[0], sibling)
        ring(1)

    rq, rk, values_t, silu_t = projected(proj, 4, 0, share_first_out)
    gated = retained(rq, rk, values_t, silu_t, 5, 0, lambda: ring(2))
    wait_bytes(wo0.at[other], sib_r.at[0])
    for d in range(DP):
        term = jnp.dot(gated, wo0[d % 2, d // 2], preferred_element_type=f32)
        for h in range(2):
            for k in range(2):
                p6s[32 * h + 2 * d + k] = term[8 * h : 8 * h + 8, DK * k : DK * k + DK].astype(bf16)
    for peer in tp_peers:
        push(p6s.at[peer], p6r.at[tp], 6, peer, dp)
    p6r[tp] = p6s[tp]
    ring(3)

    @pl.when(dp != res_owner)
    def _():
        wait_bytes(res, rs.at[3])

    landed(p6r.at[pl.ds(0, TP - 1)], 6)
    xb[...] = (res[...].astype(f32) + jnp.sum(p6r[...].astype(f32), axis=0)).astype(bf16)

    for peer in tp_peers:
        push(xb, xg1.at[tp], 7, peer, dp)
    xg1[tp] = xb[...]
    ring(4)
    wait_bytes(w1.at[other], sib_r.at[1])
    landed(xg1.at[pl.ds(0, TP - 1)], 7)

    def features(d):
        halves = [
            jnp.concatenate([xg1[32 * h + 2 * d + k].astype(f32) for k in range(2)], axis=1)
            for h in range(2)
        ]
        return jnp.concatenate(halves, axis=0)

    squares = jnp.zeros((SEQ, FEATS), f32)
    total = jnp.zeros((SEQ, DK), f32)
    for d in range(DP):
        xf = features(d)
        squares = squares + xf * xf
        total = total + lax.dot_general(
            xf.astype(bf16), w1[d % 2, d // 2, 0:DK], (((1,), (1,)), ((), ())),
            preferred_element_type=f32,
        )
    squares = jnp.sum(squares, axis=1, keepdims=True)
    proj = (total * lax.rsqrt(squares / D + norm_eps)).astype(bf16)
    rq, rk, values_t, silu_t = projected(proj, 8, 1, lambda: None)
    gated = retained(rq, rk, values_t, silu_t, 9, 1, lambda: None)
    for d in range(DP):
        term = jnp.dot(gated, w1[d % 2, d // 2, DK:WIDE], preferred_element_type=f32)
        xf = features(d)
        for j in range(ROWS):
            block = slice(ROWS * j, ROWS * j + ROWS)
            own = jnp.where(tp == DP * j + d, xf[block], 0.0)
            pfs[j, d] = (term[block] + own).astype(bf16)
    for peer in dp_peers:
        for j in range(ROWS):
            push(pfs.at[j, peer], pfr.at[tp], 10, ROWS * dp + j, peer)
    for j in range(ROWS):
        here = tp == ROWS * dp + j

        @pl.when(here)
        def _():
            pltpu.make_async_copy(pfs.at[j, dp], pfr.at[tp], rs.at[10]).start()

        @pl.when(jnp.logical_not(here))
        def _():
            push(pfs.at[j, dp], pfr.at[tp], 10, ROWS * dp + j, dp)

    wait_bytes(pfr, rs.at[10])
    out[...] = jnp.sum(pfr[...].astype(f32), axis=0).astype(bf16)

    for ref, sem_id in sends:
        wait_bytes(ref, ss.at[sem_id])

    @pl.when(dp == res_owner)
    def _():
        wait_bytes(res_s.at[pl.ds(0, DP - 1)], ss.at[3])

    @pl.when(lax.div(tp, ROWS) == dp)
    def _():
        wait_bytes(pfr.at[pl.ds(0, TP - 1)], ss.at[10])

    @pl.when(lax.div(tp, ROWS) != dp)
    def _():
        wait_bytes(pfr, ss.at[10])

    wait_bytes(wo0.at[0, pl.ds(0, RING - 1)], side_s)
    wait_bytes(wo0.at[0], side_s)
    wait_bytes(w1.at[0, pl.ds(0, RING - 1)], side_s)
    wait_bytes(w1.at[0], side_s)


def body(tokens, lengths, states, norm_gain, w_query, w_key, w_value, w_gate, head_gain, w_out):
    flip = lambda w: jnp.transpose(w, (0, 2, 1))
    hbm = pl.BlockSpec(memory_space=pl.ANY)
    vmem = pltpu.VMEM
    dma = pltpu.SemaphoreType.DMA
    return pl.pallas_call(
        kernel,
        out_shape=(vmem((ROWS, FEATS), bf16), vmem(states.shape, f32)),
        in_specs=[hbm] * 10,
        out_specs=(pl.BlockSpec(memory_space=vmem), pl.BlockSpec(memory_space=vmem)),
        scratch_shapes=[
            pltpu.SMEM((SEQ,), jnp.int32),
            vmem((ROWS, FEATS), bf16),
            vmem((TP, ROWS, FEATS), bf16),
            vmem((TP * ROWS, FEATS), bf16),
            vmem((DK, FEATS), bf16),
            vmem((DK, FEATS), bf16),
            vmem((2, RING, COLS, FEATS), bf16),
            vmem((2, RING, WIDE, FEATS), bf16),
            vmem((LAYERS, FEATS), bf16),
            vmem((LAYERS, COLS), bf16),
            vmem((DP, SEQ, DK), bf16),
            vmem((DP, SEQ, DK), bf16),
            vmem((DP, 1, DK), f32),
            vmem((DP, 1, DK), f32),
            vmem((LAYERS, GROUP, SEQ, DK), bf16),
            vmem((LAYERS, 2, DK), f32),
            vmem((LAYERS, GROUP, 2, DK), f32),
            vmem((DP, 8, DK), bf16),
            vmem((8, DK), bf16),
            vmem((TP, 8, DK), bf16),
            vmem((TP, 8, DK), bf16),
            vmem((8, DK), bf16),
            vmem((TP, 8, DK), bf16),
            vmem((ROWS, DP, ROWS, FEATS), bf16),
            vmem((TP, ROWS, FEATS), bf16),
            dma((15,)),
            dma((4,)),
            dma((3,)),
            dma((3,)),
            dma,
            dma((11,)),
            dma((11,)),
        ],
        compiler_params=pltpu.CompilerParams(collective_id=0, has_side_effects=True),
        name="retention_step",
    )(
        tokens, lengths, states, norm_gain,
        flip(w_query), flip(w_key), flip(w_value), flip(w_gate), head_gain, w_out,
    )


def solution(mesh):
    placed = (
        P("tp", "dp"),
        P("dp"),
        P(None, "dp", "tp", None),
        P(None, "dp"),
        P(None, "dp", "tp"),
        P(None, "dp", "tp"),
        P(None, "dp", "tp"),
        P(None, "dp", "tp"),
        P(None, "tp"),
        P(None, "tp", "dp"),
    )
    return jax.shard_map(
        body,
        mesh=mesh,
        in_specs=placed,
        out_specs=(P("tp", "dp"), P(None, "dp", "tp", None)),
        check_vma=False,
    )
```

time: 95.2 us -> 80.1 us (0.84)
  Pallas kernels: 91.2 us -> 78 us
  local copies, waits for them, and re-layouts: 3.11 us -> 1.37 us
    pallas_call x1, Pallas kernels: 91.2 us -> 78 us  [body(): pl.pallas_call(kernel, out_shape=(vmem((ROWS, FEATS), bf16), vmem(states....]
    unnamed x4 -> x2, local copies, waits for them, and re-layouts: 3.11 us -> 1.37 us
where the time goes in v2:
time: 80.1 us; the launch traced here: 80 us
  Pallas kernels  78 us (97%)
  local copies, waits for them, and re-layouts  1.37 us (2%)
    pallas_call x1, Pallas kernels, body(): pl.pallas_call(kernel, out_shape=(vmem((ROWS, FEATS), bf16), vmem(states....  78 us

profile of v2, /device:TPU:1, one launch (start us, length us, event | category | flops | bytes accessed | tf_op | source)
XLA Modules:
  0.0 80.0 jit_solution(16354155121735993775)
XLA Ops:
  0.6 78.0 %retention_step.1 = (bf16[4,256]{1,0:T(4,128)(2,1)S(1)}, f32[2,16,32,128]{3,2,1,0:T(8,128)S(1)}) custom-call(bf16[4,256]{1,0:T(4,128)(2,1)} %tok.1, s32[16]{0:T(128)} %lens.1, f32[2,16,32,128]{3,2,1,0:T(8,128)} %states.1, bf16[2,256]{1,0:T(2,128)(2,1)} %ngain.1, bf16[2,32,256]{2,1,0:T(8,128)(2,1)} %bitcast.4, bf16[2,32,256]{2,1,0:T(8,128)(2,1)} %bitcast.5, ...), custom_call_target="tpu_custom_call" | custom-call | tf_op jit(solution)/shard_map/retention_step/pallas_call | solution.py:339
  78.6 0.6 copy.14
  79.2 0.8 copy.15

commit v3 on v2

--- a/solution.py
+++ b/solution.py
@@ -18,7 +18,9 @@
 SEQ = 16
 GROUP = 4
 FAR = (4, 5, 3, 6, 2, 7, 1, 0)
-WIDE = DK + COLS
+PIECES = 11
+VALUE, OUT = 8, 10
+CUT = 6
 
 norm_eps = 1e-06
 group_eps = 1e-05
@@ -59,31 +61,123 @@
     dp_peers = [xo2[o] * 2 + (other if c else core) for o, c in line]
     group_peers = [grp * GROUP + lax.rem(gj + k, GROUP) for k in (3, 2, 1)]
 
+    load_tok = pltpu.make_async_copy(tok, xo, lsem.at[0])
+    load_out = pltpu.make_async_copy(wout.at[0], wo0.at[core, xc], lsem.at[1])
     loads = [
-        pltpu.make_async_copy(tok, xo, lsem.at[0]),
-        pltpu.make_async_copy(wout.at[0], wo0.at[core, xc], lsem.at[1]),
-        pltpu.make_async_copy(wq.at[1], wp1.at[0:32], lsem.at[2]),
-        pltpu.make_async_copy(wk.at[1], wp1.at[32:64], lsem.at[3]),
-        pltpu.make_async_copy(wv.at[1], wp1.at[64:96], lsem.at[4]),
-        pltpu.make_async_copy(wg.at[1], wp1.at[96:128], lsem.at[5]),
-        pltpu.make_async_copy(wout.at[1], w1.at[core, xc, DK:WIDE], lsem.at[6]),
-        pltpu.make_async_copy(ngain, ng, lsem.at[7]),
         pltpu.make_async_copy(wq.at[0], wp0.at[0:32], lsem.at[8]),
         pltpu.make_async_copy(wk.at[0], wp0.at[32:64], lsem.at[9]),
         pltpu.make_async_copy(wv.at[0], wp0.at[64:96], lsem.at[10]),
         pltpu.make_async_copy(wg.at[0], wp0.at[96:128], lsem.at[11]),
+        pltpu.make_async_copy(wq.at[1], wp1.at[0], lsem.at[2]),
+        pltpu.make_async_copy(wk.at[1], wp1.at[1], lsem.at[3]),
+        pltpu.make_async_copy(wv.at[1], wp1.at[2], lsem.at[4]),
+        pltpu.make_async_copy(wg.at[1], wp1.at[3], lsem.at[5]),
+        pltpu.make_async_copy(wout.at[1], w1.at[core, xc, OUT], lsem.at[6]),
+        pltpu.make_async_copy(ngain, ng, lsem.at[7]),
         pltpu.make_async_copy(lens, len_s, lsem.at[12]),
         pltpu.make_async_copy(hgain, hg, lsem.at[13]),
         pltpu.make_async_copy(states, st, lsem.at[14]),
     ]
+    load_tok.start()
     barrier = pltpu.get_barrier_semaphore()
     for peer in tp_peers:
         pl.semaphore_signal(barrier, inc=1, device_id=(peer, dp), device_id_type=MESH)
     for peer in dp_peers:
         pl.semaphore_signal(barrier, inc=1, device_id=(tp, peer), device_id_type=MESH)
+    load_out.start()
     for c in loads:
         c.start()
-
+    load_tok.wait()
+    pl.semaphore_wait(barrier, TP + DP - 2)
+
+    sends = []
+
+    def push(src, dst, sem_id, peer_tp, peer_dp):
+        pltpu.make_async_remote_copy(
+            src_ref=src, dst_ref=dst, send_sem=ss.at[sem_id], recv_sem=rs.at[sem_id],
+            device_id=(peer_tp, peer_dp), device_id_type=MESH,
+        ).start()
+
+    def push_side(src, dst, recv, peer_dp):
+        pltpu.make_async_remote_copy(
+            src_ref=src, dst_ref=dst, send_sem=side_s, recv_sem=recv,
+            device_id=(tp, peer_dp), device_id_type=MESH,
+        ).start()
+
+    def send_group(src, dst, sem_id):
+        for peer in group_peers:
+            push(src, dst, sem_id, peer, dp)
+
+    def wait_bytes(ref, sem):
+        pltpu.make_async_copy(ref, ref, sem).wait()
+
+    def landed(ref, sem_id):
+        wait_bytes(ref, rs.at[sem_id])
+        sends.append((ref, sem_id))
+
+    right, left, sibling = xo2[1] * 2 + core, xo2[7] * 2 + core, xc * 2 + other
+
+    def ring(step):
+        came_right, came_left = xo2[(RING - step) % RING], xo2[step]
+        if step == 0:
+            landed(w1.at[core, xc, pl.ds(0, 2 * GROUP - 2)], 8)
+        elif step < 4:
+            wait_bytes(w1.at[core, came_right], ring_r.at[step - 1])
+            wait_bytes(w1.at[core, came_left], ring_l.at[step - 1])
+        else:
+            wait_bytes(w1.at[core, came_right, pl.ds(0, CUT)], ring_r.at[3])
+            wait_bytes(w1.at[core, came_left, pl.ds(CUT, PIECES - CUT)], ring_l.at[3])
+        if step < 3:
+            push_side(w1.at[core, came_right], w1.at[core, came_right], ring_r.at[step], right)
+            push_side(w1.at[core, came_left], w1.at[core, came_left], ring_l.at[step], left)
+        if step == 3:
+            part_r = w1.at[core, came_right, pl.ds(0, CUT)]
+            part_l = w1.at[core, came_left, pl.ds(CUT, PIECES - CUT)]
+            push_side(part_r, part_r, ring_r.at[3], right)
+            push_side(part_l, part_l, ring_l.at[3], left)
+        push_side(w1.at[core, came_right], w1.at[core, came_right], sib_r.at[1], sibling)
+        if 1 <= step <= 3:
+            push_side(w1.at[core, came_left], w1.at[core, came_left], sib_r.at[1], sibling)
+
+    def columns(values_gates):
+        both_t = jnp.transpose(jnp.concatenate([values_gates, pad_rows], axis=0))
+        values_t, gate_t = both_t[0:COLS, :], both_t[COLS : 2 * COLS, :]
+        return values_t, gate_t / (1.0 + jnp.exp(-gate_t))
+
+    def rotated(query, key):
+        rq = query * cosine + pltpu.roll(query, half, 1) * sine
+        rk = (key * cosine + pltpu.roll(key, half, 1) * sine) * DK ** (-0.5)
+        return rq, rk
+
+    def retained(rq, rk, values_t, silu_t, sem_id, l, meanwhile):
+        read = jnp.zeros((COLS, DK), f32)
+        for s in range(SEQ):
+            r = jnp.sum(st[l, s] * rq[s : s + 1, :], axis=1, keepdims=True)
+            read = jnp.where(lane32 == s, r, read)
+        match = jnp.sum(rq * rk, axis=1, keepdims=True)
+        match = jnp.sum(jnp.where(diag, match, 0.0), axis=0, keepdims=True)
+        read = gamma * read + values_t * match
+        sts[l, 0:1] = jnp.sum(read, axis=0, keepdims=True)
+        sts[l, 1:2] = jnp.sum(read * read, axis=0, keepdims=True)
+        send_group(sts.at[l], str_.at[l, gj], sem_id)
+        str_[l, gj] = sts[l]
+        for s in range(SEQ):
+            st[l, s] = gamma * st[l, s] + values_t[:, s : s + 1] * rk[s : s + 1, :]
+        meanwhile()
+        landed(str_.at[l, pl.ds(0, GROUP - 1)], sem_id)
+        both = (str_[l, 0] + str_[l, 1]) + (str_[l, 2] + str_[l, 3])
+        mean_v = both[0:1, :] / DK
+        square = both[1:2, :] / DK
+        grouped = (read - mean_v) * lax.rsqrt(square - mean_v * mean_v + group_eps) * hgains[l]
+        gated = jnp.concatenate([silu_t * grouped, jnp.zeros((DK - COLS, DK), f32)], axis=0)
+        return jnp.transpose(gated)[0:SEQ, 0:COLS].astype(bf16)
+
+    for peer in tp_peers:
+        push(xo, xg.at[tp], 0, peer, dp)
+    xg[tp] = xo[...]
+    load_out.wait()
+    for o in FAR[:7]:
+        push_side(wo0.at[core, xc], wo0.at[core, xc], sib_r.at[2], xo2[o] * 2 + core)
     for c in loads:
         c.wait()
     row = lax.broadcasted_iota(jnp.int32, (SEQ, DK), 0)
@@ -109,97 +203,9 @@
         for l in range(LAYERS)
     ]
     pad_rows = jnp.zeros((DK - SEQ, DK), f32)
-    w1[core, xc, 0:DK] = (wp1[...].astype(f32) * ng[1:2, :].astype(f32)).astype(bf16)
-
-    pl.semaphore_wait(barrier, TP + DP - 2)
-
-    sends = []
-
-    def push(src, dst, sem_id, peer_tp, peer_dp):
-        pltpu.make_async_remote_copy(
-            src_ref=src, dst_ref=dst, send_sem=ss.at[sem_id], recv_sem=rs.at[sem_id],
-            device_id=(peer_tp, peer_dp), device_id_type=MESH,
-        ).start()
-
-    def push_side(src, dst, recv, peer_dp):
-        pltpu.make_async_remote_copy(
-            src_ref=src, dst_ref=dst, send_sem=side_s, recv_sem=recv,
-            device_id=(tp, peer_dp), device_id_type=MESH,
-        ).start()
-
-    def send_group(src, dst, sem_id):
-        for peer in group_peers:
-            push(src, dst, sem_id, peer, dp)
-
-    def wait_bytes(ref, sem):
-        pltpu.make_async_copy(ref, ref, sem).wait()
-
-    def landed(ref, sem_id):
-        wait_bytes(ref, rs.at[sem_id])
-        sends.append((ref, sem_id))
-
-    right, left, sibling = xo2[1] * 2 + core, xo2[7] * 2 + core, xc * 2 + other
-
-    def ring(step):
-        came_right, came_left = xo2[(RING - step) % RING], xo2[step]
-        if 1 <= step <= 4:
-            wait_bytes(w1.at[core, came_right], ring_r.at[step - 1])
-        if 1 <= step <= 3:
-            wait_bytes(w1.at[core, came_left], ring_l.at[step - 1])
-        if step <= 3:
-            push_side(w1.at[core, came_right], w1.at[core, came_right], ring_r.at[step], right)
-        if step <= 2:
-            push_side(w1.at[core, came_left], w1.at[core, came_left], ring_l.at[step], left)
-        if step == 4:
-            push_side(w1.at[core], w1.at[core], sib_r.at[1], sibling)
-
-    def projected(proj, sem_id, l, meanwhile):
-        pj[l, gj] = proj
-        send_group(pj.at[l, gj], pj.at[l, gj], sem_id)
-        proj_t = jnp.transpose(jnp.concatenate([proj.astype(f32), pad_rows], axis=0))
-        values_t = proj_t[64:96, :]
-        gate_t = proj_t[96:128, :]
-        silu_t = gate_t / (1.0 + jnp.exp(-gate_t))
-        meanwhile()
-        landed(pj.at[l, pl.ds(0, GROUP - 1)], sem_id)
-        query = jnp.zeros((SEQ, DK), f32)
-        key = jnp.zeros((SEQ, DK), f32)
-        for j in range(GROUP):
-            piece = pj[l, j].astype(f32)
-            here = lax.div(lane, 32) == j
-            query = jnp.where(here, pltpu.roll(piece, 32 * j, 1) if j else piece, query)
-            shift = (32 * j - 32) % DK
-            key = jnp.where(here, pltpu.roll(piece, shift, 1) if shift else piece, key)
-        rq = query * cosine + pltpu.roll(query, half, 1) * sine
-        rk = (key * cosine + pltpu.roll(key, half, 1) * sine) * DK ** (-0.5)
-        return rq, rk, values_t, silu_t
-
-    def retained(rq, rk, values_t, silu_t, sem_id, l, meanwhile):
-        read = jnp.zeros((COLS, DK), f32)
-        for s in range(SEQ):
-            new = gamma * st[l, s] + values_t[:, s : s + 1] * rk[s : s + 1, :]
-            st[l, s] = new
-            r = jnp.sum(new * rq[s : s + 1, :], axis=1, keepdims=True)
-            read = jnp.where(lane32 == s, r, read)
-        sts[l, 0:1] = jnp.sum(read, axis=0, keepdims=True)
-        sts[l, 1:2] = jnp.sum(read * read, axis=0, keepdims=True)
-        send_group(sts.at[l], str_.at[l, gj], sem_id)
-        str_[l, gj] = sts[l]
-        meanwhile()
-        landed(str_.at[l, pl.ds(0, GROUP - 1)], sem_id)
-        both = (str_[l, 0] + str_[l, 1]) + (str_[l, 2] + str_[l, 3])
-        mean_v = both[0:1, :] / DK
-        square = both[1:2, :] / DK
-        grouped = (read - mean_v) * lax.rsqrt(square - mean_v * mean_v + group_eps) * hgains[l]
-        gated = jnp.concatenate([silu_t * grouped, jnp.zeros((DK - COLS, DK), f32)], axis=0)
-        return jnp.transpose(gated)[0:SEQ, 0:COLS].astype(bf16)
-
-    for peer in tp_peers:
-        push(xo, xg.at[tp], 0, peer, dp)
-    xg[tp] = xo[...]
-    for o in FAR[:7]:
-        push_side(wo0.at[core, xc], wo0.at[core, xc], sib_r.at[2], xo2[o] * 2 + core)
-    ring(0)
+    gain = ng[1:2, :].astype(f32)
+    for piece, n in ((gj, 0), (GROUP + gj, 1), (VALUE, 2), (VALUE + 1, 3)):
+        w1[core, xc, piece] = (wp1[n].astype(f32) * gain).astype(bf16)
     landed(xg.at[pl.ds(0, TP - 1)], 0)
     gain = ng[0:1, :].astype(f32)
     res_half, res_side = lax.div(tp, 32), lax.rem(tp, 2)
@@ -217,6 +223,8 @@
     for peer in dp_peers:
         push(p2s.at[peer], p2r.at[dp], 1, tp, peer)
         push(sqs.at[peer], sqr.at[dp], 2, tp, peer)
+    for piece in (gj, GROUP + gj):
+        send_group(w1.at[core, xc, piece], w1.at[core, xc, piece], 8)
     p2r[dp] = p2s[dp]
     sqr[dp] = sqs[dp]
     res_owner = lax.rem(lax.div(tp, 2), DP)
@@ -234,13 +242,23 @@
     squares = jnp.sum(jnp.where(diag, squares, 0.0), axis=1, keepdims=True)
     proj = (total * lax.rsqrt(squares / D + norm_eps)).astype(bf16)
 
-    def share_first_out():
-        wait_bytes(wo0.at[core, pl.ds(0, RING - 1)], sib_r.at[2])
-        push_side(wo0.at[core], wo0.at[core], sib_r.at[0], sibling)
-        ring(1)
-
-    rq, rk, values_t, silu_t = projected(proj, 4, 0, share_first_out)
-    gated = retained(rq, rk, values_t, silu_t, 5, 0, lambda: ring(2))
+    pj[gj] = proj
+    send_group(pj.at[gj], pj.at[gj], 4)
+    values_t, silu_t = columns(pltpu.roll(proj.astype(f32), 2 * COLS, 1))
+    wait_bytes(wo0.at[core, pl.ds(0, RING - 1)], sib_r.at[2])
+    push_side(wo0.at[core], wo0.at[core], sib_r.at[0], sibling)
+    ring(0)
+    landed(pj.at[pl.ds(0, GROUP - 1)], 4)
+    query = jnp.zeros((SEQ, DK), f32)
+    key = jnp.zeros((SEQ, DK), f32)
+    for j in range(GROUP):
+        piece = pj[j].astype(f32)
+        here = lax.div(lane, COLS) == j
+        query = jnp.where(here, pltpu.roll(piece, COLS * j, 1) if j else piece, query)
+        shift = (COLS * j - COLS) % DK
+        key = jnp.where(here, pltpu.roll(piece, shift, 1) if shift else piece, key)
+    rq, rk = rotated(query, key)
+    gated = retained(rq, rk, values_t, silu_t, 5, 0, lambda: ring(1))
     wait_bytes(wo0.at[other], sib_r.at[0])
     for d in range(DP):
         term = jnp.dot(gated, wo0[d % 2, d // 2], preferred_element_type=f32)
@@ -250,7 +268,7 @@
     for peer in tp_peers:
         push(p6s.at[peer], p6r.at[tp], 6, peer, dp)
     p6r[tp] = p6s[tp]
-    ring(3)
+    ring(2)
 
     @pl.when(dp != res_owner)
     def _():
@@ -262,8 +280,8 @@
     for peer in tp_peers:
         push(xb, xg1.at[tp], 7, peer, dp)
     xg1[tp] = xb[...]
+    ring(3)
     ring(4)
-    wait_bytes(w1.at[other], sib_r.at[1])
     landed(xg1.at[pl.ds(0, TP - 1)], 7)
 
     def features(d):
@@ -274,20 +292,25 @@
         return jnp.concatenate(halves, axis=0)
 
     squares = jnp.zeros((SEQ, FEATS), f32)
-    total = jnp.zeros((SEQ, DK), f32)
-    for d in range(DP):
-        xf = features(d)
-        squares = squares + xf * xf
-        total = total + lax.dot_general(
-            xf.astype(bf16), w1[d % 2, d // 2, 0:DK], (((1,), (1,)), ((), ())),
-            preferred_element_type=f32,
-        )
+    total = jnp.zeros((SEQ, COLS * OUT), f32)
+    for c in (core, other):
+        if c is other:
+            wait_bytes(w1.at[other], sib_r.at[1])
+        for o in range(RING):
+            xf = features(2 * o + c)
+            squares = squares + xf * xf
+            total = total + lax.dot_general(
+                xf.astype(bf16), w1[c, o, 0:OUT].reshape(COLS * OUT, FEATS),
+                (((1,), (1,)), ((), ())), preferred_element_type=f32,
+            )
     squares = jnp.sum(squares, axis=1, keepdims=True)
-    proj = (total * lax.rsqrt(squares / D + norm_eps)).astype(bf16)
-    rq, rk, values_t, silu_t = projected(proj, 8, 1, lambda: None)
+    proj = (total * lax.rsqrt(squares / D + norm_eps)).astype(bf16).astype(f32)
+    rq, rk = rotated(proj[:, 0:DK], proj[:, DK : 2 * DK])
+    tail = jnp.concatenate([proj[:, 2 * DK :], jnp.zeros((SEQ, DK - 2 * COLS), f32)], axis=1)
+    values_t, silu_t = columns(tail)
     gated = retained(rq, rk, values_t, silu_t, 9, 1, lambda: None)
     for d in range(DP):
-        term = jnp.dot(gated, w1[d % 2, d // 2, DK:WIDE], preferred_element_type=f32)
+        term = jnp.dot(gated, w1[d % 2, d // 2, OUT], preferred_element_type=f32)
         xf = features(d)
         for j in range(ROWS):
             block = slice(ROWS * j, ROWS * j + ROWS)
@@ -347,16 +370,16 @@
             vmem((TP, ROWS, FEATS), bf16),
             vmem((TP * ROWS, FEATS), bf16),
             vmem((DK, FEATS), bf16),
-            vmem((DK, FEATS), bf16),
+            vmem((4, COLS, FEATS), bf16),
             vmem((2, RING, COLS, FEATS), bf16),
-            vmem((2, RING, WIDE, FEATS), bf16),
+            vmem((2, RING, PIECES, COLS, FEATS), bf16),
             vmem((LAYERS, FEATS), bf16),
             vmem((LAYERS, COLS), bf16),
             vmem((DP, SEQ, DK), bf16),
             vmem((DP, SEQ, DK), bf16),
             vmem((DP, 1, DK), f32),
             vmem((DP, 1, DK), f32),
-            vmem((LAYERS, GROUP, SEQ, DK), bf16),
+            vmem((GROUP, SEQ, DK), bf16),
             vmem((LAYERS, 2, DK), f32),
             vmem((LAYERS, GROUP, 2, DK), f32),
             vmem((DP, 8, DK), bf16),
@@ -369,7 +392,7 @@
             vmem((TP, ROWS, FEATS), bf16),
             dma((15,)),
             dma((4,)),
-            dma((3,)),
+            dma((4,)),
             dma((3,)),
             dma,
             dma((11,)),

time: 80.1 us -> 75.7 us (0.945)
  Pallas kernels: 78 us -> 73.5 us
    pallas_call x1, Pallas kernels: 78 us -> 73.5 us  [body(): pl.pallas_call(kernel, out_shape=(vmem((ROWS, FEATS), bf16), vmem(states....]
where the time goes in v3:
time: 75.7 us; the launch traced here: 75.5 us
  Pallas kernels  73.5 us (97%)
  local copies, waits for them, and re-layouts  1.37 us (2%)
    pallas_call x1, Pallas kernels, body(): pl.pallas_call(kernel, out_shape=(vmem((ROWS, FEATS), bf16), vmem(states....  73.5 us

profile of v3, /device:TPU:1, one launch (start us, length us, event | category | flops | bytes accessed | tf_op | source)
XLA Modules:
  0.0 75.5 jit_solution(8579180789561148398)
XLA Ops:
  0.6 73.5 %retention_step.1 = (bf16[4,256]{1,0:T(4,128)(2,1)S(1)}, f32[2,16,32,128]{3,2,1,0:T(8,128)S(1)}) custom-call(bf16[4,256]{1,0:T(4,128)(2,1)} %tok.1, s32[16]{0:T(128)} %lens.1, f32[2,16,32,128]{3,2,1,0:T(8,128)} %states.1, bf16[2,256]{1,0:T(2,128)(2,1)} %ngain.1, bf16[2,32,256]{2,1,0:T(8,128)(2,1)} %bitcast.4, bf16[2,32,256]{2,1,0:T(8,128)(2,1)} %bitcast.5, ...), custom_call_target="tpu_custom_call" | custom-call | tf_op jit(solution)/shard_map/retention_step/pallas_call | solution.py:362
  74.1 0.6 copy.14
  74.7 0.8 %copy.15 = f32[2,16,32,128]{3,2,1,0:T(8,128)} copy(f32[2,16,32,128]{3,2,1,0:T(8,128)S(1)} %get-tuple-element.3) | data formatting | bytes 1048576

commit v4 on v3

--- a/solution.py
+++ b/solution.py
@@ -44,7 +44,8 @@
     tok, lens, states, ngain, wq, wk, wv, wg, hgain, wout,
     out, st,
     len_s, xo, xg, nrm, wp0, wp1, wo0, w1, ng, hg,
-    p2s, p2r, sqs, sqr, pj, sts, str_, res_s, res, p6s, p6r, xb, xg1, pfs, pfr,
+    p2s, p2r, sqs, sqr, pj, stat, stats0, stats1, res_s, res,
+    us0, ur0, xb, xg1, us1, ur1, rest_s, rest, means, vsum, vsums,
     lsem, ring_r, ring_l, sib_r, side_s, ss, rs,
 ):
     tp = lax.axis_index("tp")
@@ -149,28 +150,48 @@
         rk = (key * cosine + pltpu.roll(key, half, 1) * sine) * DK ** (-0.5)
         return rq, rk
 
-    def retained(rq, rk, values_t, silu_t, sem_id, l, meanwhile):
+    def by_sequence(channels_t):
+        full = jnp.concatenate([channels_t, jnp.zeros((DK - COLS, DK), f32)], axis=0)
+        return jnp.transpose(full)[0:SEQ, 0:COLS].astype(bf16)
+
+    def readout(rq, rk, values_t, value_mean, l):
         read = jnp.zeros((COLS, DK), f32)
         for s in range(SEQ):
             r = jnp.sum(st[l, s] * rq[s : s + 1, :], axis=1, keepdims=True)
             read = jnp.where(lane32 == s, r, read)
         match = jnp.sum(rq * rk, axis=1, keepdims=True)
+        state_mean = (means[0, l] + means[1, l]) + (means[2, l] + means[3, l])
+        mean_v = jnp.sum(rq * state_mean, axis=1, keepdims=True) * gamma[0:SEQ, 0:1]
+        mean_v = mean_v + match * value_mean
         match = jnp.sum(jnp.where(diag, match, 0.0), axis=0, keepdims=True)
-        read = gamma * read + values_t * match
-        sts[l, 0:1] = jnp.sum(read, axis=0, keepdims=True)
-        sts[l, 1:2] = jnp.sum(read * read, axis=0, keepdims=True)
-        send_group(sts.at[l], str_.at[l, gj], sem_id)
-        str_[l, gj] = sts[l]
+        mean_v = jnp.sum(jnp.where(diag, mean_v, 0.0), axis=0, keepdims=True)
+        read = gamma * read + values_t * match - mean_v
+        stat[l] = jnp.sum(read * read, axis=0, keepdims=True)
+        return read
+
+    def update(rk, values_t, l):
         for s in range(SEQ):
             st[l, s] = gamma * st[l, s] + values_t[:, s : s + 1] * rk[s : s + 1, :]
-        meanwhile()
-        landed(str_.at[l, pl.ds(0, GROUP - 1)], sem_id)
-        both = (str_[l, 0] + str_[l, 1]) + (str_[l, 2] + str_[l, 3])
-        mean_v = both[0:1, :] / DK
-        square = both[1:2, :] / DK
-        grouped = (read - mean_v) * lax.rsqrt(square - mean_v * mean_v + group_eps) * hgains[l]
-        gated = jnp.concatenate([silu_t * grouped, jnp.zeros((DK - COLS, DK), f32)], axis=0)
-        return jnp.transpose(gated)[0:SEQ, 0:COLS].astype(bf16)
+
+    t_row = lax.broadcasted_iota(jnp.int32, (TP, DK), 0)
+
+    def coefficients(ref):
+        head_sum = ref[...].reshape(TP, DK)
+        for bit in (1, 2):
+            up = lax.rem(lax.div(t_row, bit), 2) == 1
+            head_sum = head_sum + jnp.where(
+                up, pltpu.roll(head_sum, bit, 0), pltpu.roll(head_sum, TP - bit, 0)
+            )
+        scale = lax.rsqrt(head_sum / DK + group_eps)
+        return jnp.transpose(jnp.concatenate([scale, scale], axis=0))
+
+    def scaled(coef, ref):
+        acc = None
+        for g in range(0, TP, GROUP):
+            part = [ref[g + j].astype(f32) for j in range(GROUP)]
+            part = coef[:, g : g + 1] * ((part[0] + part[1]) + (part[2] + part[3]))
+            acc = part if acc is None else acc + part
+        return acc
 
     for peer in tp_peers:
         push(xo, xg.at[tp], 0, peer, dp)
@@ -206,6 +227,12 @@
     gain = ng[1:2, :].astype(f32)
     for piece, n in ((gj, 0), (GROUP + gj, 1), (VALUE, 2), (VALUE + 1, 3)):
         w1[core, xc, piece] = (wp1[n].astype(f32) * gain).astype(bf16)
+    vsum[gj] = jnp.sum(w1[core, xc, VALUE].astype(f32), axis=0, keepdims=True)
+    for l in range(LAYERS):
+        means[gj, l] = jnp.sum(st[l], axis=1) / DK
+    send_group(vsum.at[gj], vsum.at[gj], 5)
+    for piece in (gj, GROUP + gj):
+        send_group(w1.at[core, xc, piece], w1.at[core, xc, piece], 8)
     landed(xg.at[pl.ds(0, TP - 1)], 0)
     gain = ng[0:1, :].astype(f32)
     res_half, res_side = lax.div(tp, 32), lax.rem(tp, 2)
@@ -223,8 +250,7 @@
     for peer in dp_peers:
         push(p2s.at[peer], p2r.at[dp], 1, tp, peer)
         push(sqs.at[peer], sqr.at[dp], 2, tp, peer)
-    for piece in (gj, GROUP + gj):
-        send_group(w1.at[core, xc, piece], w1.at[core, xc, piece], 8)
+    send_group(means.at[gj], means.at[gj], 9)
     p2r[dp] = p2s[dp]
     sqr[dp] = sqs[dp]
     res_owner = lax.rem(lax.div(tp, 2), DP)
@@ -235,6 +261,13 @@
             push(res_s.at[peer], res, 3, tp, peer)
         res[...] = res_s[dp]
 
+    wait_bytes(wo0.at[core, pl.ds(0, RING - 1)], sib_r.at[2])
+    push_side(wo0.at[core], wo0.at[core], sib_r.at[0], sibling)
+    ring(0)
+    landed(vsum.at[pl.ds(0, GROUP - 1)], 5)
+    vsums[dp] = (vsum[0] + vsum[1]) + (vsum[2] + vsum[3])
+    for peer in dp_peers:
+        push(vsums.at[dp], vsums.at[dp], 14, tp, peer)
     landed(p2r.at[pl.ds(0, DP - 1)], 1)
     landed(sqr.at[pl.ds(0, DP - 1)], 2)
     total = jnp.sum(p2r[...].astype(f32), axis=0)
@@ -245,37 +278,54 @@
     pj[gj] = proj
     send_group(pj.at[gj], pj.at[gj], 4)
     values_t, silu_t = columns(pltpu.roll(proj.astype(f32), 2 * COLS, 1))
-    wait_bytes(wo0.at[core, pl.ds(0, RING - 1)], sib_r.at[2])
-    push_side(wo0.at[core], wo0.at[core], sib_r.at[0], sibling)
-    ring(0)
+    wait_bytes(wo0.at[other], sib_r.at[0])
+
+    def first_blocks(left_side, ref):
+        for d in range(DP):
+            term = jnp.dot(left_side, wo0[d % 2, d // 2], preferred_element_type=f32)
+            for h in range(2):
+                for k in range(2):
+                    ref[32 * h + 2 * d + k] = term[
+                        8 * h : 8 * h + 8, DK * k : DK * k + DK
+                    ].astype(bf16)
+
+    weight_t = silu_t * hgains[0]
+    ring(1)
+    landed(means.at[pl.ds(0, GROUP - 1)], 9)
     landed(pj.at[pl.ds(0, GROUP - 1)], 4)
+    value_mean = jnp.zeros((SEQ, DK), f32)
     query = jnp.zeros((SEQ, DK), f32)
     key = jnp.zeros((SEQ, DK), f32)
     for j in range(GROUP):
         piece = pj[j].astype(f32)
+        value_mean = value_mean + piece
         here = lax.div(lane, COLS) == j
         query = jnp.where(here, pltpu.roll(piece, COLS * j, 1) if j else piece, query)
         shift = (COLS * j - COLS) % DK
         key = jnp.where(here, pltpu.roll(piece, shift, 1) if shift else piece, key)
     rq, rk = rotated(query, key)
-    gated = retained(rq, rk, values_t, silu_t, 5, 0, lambda: ring(1))
-    wait_bytes(wo0.at[other], sib_r.at[0])
-    for d in range(DP):
-        term = jnp.dot(gated, wo0[d % 2, d // 2], preferred_element_type=f32)
-        for h in range(2):
-            for k in range(2):
-                p6s[32 * h + 2 * d + k] = term[8 * h : 8 * h + 8, DK * k : DK * k + DK].astype(bf16)
+    is_value = lax.div(lane, COLS) == 2
+    value_mean = jnp.sum(jnp.where(is_value, value_mean, 0.0), axis=1, keepdims=True) / DK
+    read = readout(rq, rk, values_t, value_mean, 0)
     for peer in tp_peers:
-        push(p6s.at[peer], p6r.at[tp], 6, peer, dp)
-    p6r[tp] = p6s[tp]
+        push(stat.at[0], stats0.at[tp], 11, peer, dp)
+    first_blocks(by_sequence(weight_t * read), us0)
+    for peer in tp_peers:
+        push(us0.at[peer], ur0.at[tp], 6, peer, dp)
+    stats0[tp] = stat[0]
+    ur0[tp] = us0[tp]
+    update(rk, values_t, 0)
     ring(2)
-
+    landed(stats0.at[pl.ds(0, TP - 1)], 11)
+    coef = coefficients(stats0)
+    coef = jnp.where(res_half == 1, coef[8:16], coef[0:8])
     @pl.when(dp != res_owner)
     def _():
         wait_bytes(res, rs.at[3])
 
-    landed(p6r.at[pl.ds(0, TP - 1)], 6)
-    xb[...] = (res[...].astype(f32) + jnp.sum(p6r[...].astype(f32), axis=0)).astype(bf16)
+    base = res[...].astype(f32)
+    landed(ur0.at[pl.ds(0, TP - 1)], 6)
+    xb[...] = (base + scaled(coef, ur0)).astype(bf16)
 
     for peer in tp_peers:
         push(xb, xg1.at[tp], 7, peer, dp)
@@ -291,47 +341,82 @@
         ]
         return jnp.concatenate(halves, axis=0)
 
+    rest_j, rest_d = lax.div(tp, DP), lax.rem(tp, DP)
+    rest_tp = ROWS * dp + rest_j
+    rest_at = 32 * lax.div(rest_j, 2) + 2 * rest_d
+    piece = jnp.concatenate([xg1[rest_at + k].astype(f32) for k in range(2)], axis=1)
+    rest_s[...] = jnp.where(lax.rem(rest_j, 2) == 1, piece[4:8], piece[0:4]).astype(bf16)
+    rest_here = jnp.logical_and(tp == rest_tp, dp == rest_d)
+
+    @pl.when(rest_here)
+    def _():
+        pltpu.make_async_copy(rest_s, rest, rs.at[13]).start()
+
+    @pl.when(jnp.logical_not(rest_here))
+    def _():
+        push(rest_s, rest, 13, rest_tp, rest_d)
+
     squares = jnp.zeros((SEQ, FEATS), f32)
     total = jnp.zeros((SEQ, COLS * OUT), f32)
+    value_sum = jnp.zeros((SEQ, FEATS), f32)
+    landed(vsums.at[pl.ds(0, DP - 1)], 14)
     for c in (core, other):
         if c is other:
             wait_bytes(w1.at[other], sib_r.at[1])
         for o in range(RING):
             xf = features(2 * o + c)
             squares = squares + xf * xf
+            value_sum = value_sum + xf * vsums[2 * o + c]
             total = total + lax.dot_general(
                 xf.astype(bf16), w1[c, o, 0:OUT].reshape(COLS * OUT, FEATS),
                 (((1,), (1,)), ((), ())), preferred_element_type=f32,
             )
     squares = jnp.sum(squares, axis=1, keepdims=True)
-    proj = (total * lax.rsqrt(squares / D + norm_eps)).astype(bf16).astype(f32)
+    row_scale = lax.rsqrt(squares / D + norm_eps)
+    value_mean = jnp.sum(value_sum, axis=1, keepdims=True) * row_scale / DK
+    proj = (total * row_scale).astype(bf16).astype(f32)
     rq, rk = rotated(proj[:, 0:DK], proj[:, DK : 2 * DK])
     tail = jnp.concatenate([proj[:, 2 * DK :], jnp.zeros((SEQ, DK - 2 * COLS), f32)], axis=1)
     values_t, silu_t = columns(tail)
-    gated = retained(rq, rk, values_t, silu_t, 9, 1, lambda: None)
-    for d in range(DP):
-        term = jnp.dot(gated, w1[d % 2, d // 2, OUT], preferred_element_type=f32)
-        xf = features(d)
+
+    def last_blocks(left_side, ref):
+        for d in range(DP):
+            term = jnp.dot(left_side, w1[d % 2, d // 2, OUT], preferred_element_type=f32)
+            for j in range(ROWS):
+                ref[j, d] = term[ROWS * j : ROWS * j + ROWS].astype(bf16)
+
+    def push_last(src_of, dst, sem_id):
+        for peer in dp_peers:
+            for j in range(ROWS):
+                push(src_of(j, peer), dst, sem_id, ROWS * dp + j, peer)
         for j in range(ROWS):
-            block = slice(ROWS * j, ROWS * j + ROWS)
-            own = jnp.where(tp == DP * j + d, xf[block], 0.0)
-            pfs[j, d] = (term[block] + own).astype(bf16)
-    for peer in dp_peers:
-        for j in range(ROWS):
-            push(pfs.at[j, peer], pfr.at[tp], 10, ROWS * dp + j, peer)
-    for j in range(ROWS):
-        here = tp == ROWS * dp + j
-
-        @pl.when(here)
-        def _():
-            pltpu.make_async_copy(pfs.at[j, dp], pfr.at[tp], rs.at[10]).start()
-
-        @pl.when(jnp.logical_not(here))
-        def _():
-            push(pfs.at[j, dp], pfr.at[tp], 10, ROWS * dp + j, dp)
-
-    wait_bytes(pfr, rs.at[10])
-    out[...] = jnp.sum(pfr[...].astype(f32), axis=0).astype(bf16)
+            here = tp == ROWS * dp + j
+
+            @pl.when(here)
+            def _():
+                pltpu.make_async_copy(src_of(j, dp), dst, rs.at[sem_id]).start()
+
+            @pl.when(jnp.logical_not(here))
+            def _():
+                push(src_of(j, dp), dst, sem_id, ROWS * dp + j, dp)
+
+    weight_t = silu_t * hgains[1]
+    read = readout(rq, rk, values_t, value_mean, 1)
+    push_last(lambda j, peer: stat.at[1], stats1.at[tp], 12)
+    last_blocks(by_sequence(weight_t * read), us1)
+    push_last(lambda j, peer: us1.at[j, peer], ur1.at[tp], 10)
+    update(rk, values_t, 1)
+    wait_bytes(stats1, rs.at[12])
+    coef = coefficients(stats1)
+    coef = jnp.where(
+        gj < 2,
+        jnp.where(gj == 0, coef[0:4], coef[4:8]),
+        jnp.where(gj == 2, coef[8:12], coef[12:16]),
+    )
+    wait_bytes(rest, rs.at[13])
+    base = rest[...].astype(f32)
+    wait_bytes(ur1, rs.at[10])
+    out[...] = (base + scaled(coef, ur1)).astype(bf16)
 
     for ref, sem_id in sends:
         wait_bytes(ref, ss.at[sem_id])
@@ -340,13 +425,21 @@
     def _():
         wait_bytes(res_s.at[pl.ds(0, DP - 1)], ss.at[3])
 
+    last = ((ur1, 10), (stats1, 12))
+
     @pl.when(lax.div(tp, ROWS) == dp)
     def _():
-        wait_bytes(pfr.at[pl.ds(0, TP - 1)], ss.at[10])
+        for ref, sem_id in last:
+            wait_bytes(ref.at[pl.ds(0, TP - 1)], ss.at[sem_id])
 
     @pl.when(lax.div(tp, ROWS) != dp)
     def _():
-        wait_bytes(pfr, ss.at[10])
+        for ref, sem_id in last:
+            wait_bytes(ref, ss.at[sem_id])
+
+    @pl.when(jnp.logical_not(rest_here))
+    def _():
+        wait_bytes(rest, ss.at[13])
 
     wait_bytes(wo0.at[0, pl.ds(0, RING - 1)], side_s)
     wait_bytes(wo0.at[0], side_s)
@@ -380,8 +473,9 @@
             vmem((DP, 1, DK), f32),
             vmem((DP, 1, DK), f32),
             vmem((GROUP, SEQ, DK), bf16),
-            vmem((LAYERS, 2, DK), f32),
-            vmem((LAYERS, GROUP, 2, DK), f32),
+            vmem((LAYERS, 1, DK), f32),
+            vmem((TP, 1, DK), f32),
+            vmem((TP, 1, DK), f32),
             vmem((DP, 8, DK), bf16),
             vmem((8, DK), bf16),
             vmem((TP, 8, DK), bf16),
@@ -390,13 +484,18 @@
             vmem((TP, 8, DK), bf16),
             vmem((ROWS, DP, ROWS, FEATS), bf16),
             vmem((TP, ROWS, FEATS), bf16),
+            vmem((ROWS, FEATS), bf16),
+            vmem((ROWS, FEATS), bf16),
+            vmem((GROUP, LAYERS, SEQ, DK), f32),
+            vmem((GROUP, 1, FEATS), f32),
+            vmem((DP, 1, FEATS), f32),
             dma((15,)),
             dma((4,)),
             dma((4,)),
             dma((3,)),
             dma,
-            dma((11,)),
-            dma((11,)),
+            dma((15,)),
+            dma((15,)),
         ],
         compiler_params=pltpu.CompilerParams(collective_id=0, has_side_effects=True),
         name="retention_step",

time: 75.7 us -> 69.7 us (0.921)
  Pallas kernels: 73.5 us -> 67.5 us
    pallas_call x1, Pallas kernels: 73.5 us -> 67.5 us  [body(): pl.pallas_call(kernel, out_shape=(vmem((ROWS, FEATS), bf16), vmem(states....]
where the time goes in v4:
time: 69.7 us; the launch traced here: 69.5 us
  Pallas kernels  67.5 us (97%)
  local copies, waits for them, and re-layouts  1.37 us (2%)
    pallas_call x1, Pallas kernels, body(): pl.pallas_call(kernel, out_shape=(vmem((ROWS, FEATS), bf16), vmem(states....  67.5 us

profile of v4, /device:TPU:1, one launch (start us, length us, event | category | flops | bytes accessed | tf_op | source)
XLA Modules:
  0.0 69.5 jit_solution(4161943268792365833)
XLA Ops:
  0.6 67.5 %retention_step.1 = (bf16[4,256]{1,0:T(4,128)(2,1)S(1)}, f32[2,16,32,128]{3,2,1,0:T(8,128)S(1)}) custom-call(bf16[4,256]{1,0:T(4,128)(2,1)} %tok.1, s32[16]{0:T(128)} %lens.1, f32[2,16,32,128]{3,2,1,0:T(8,128)} %states.1, bf16[2,256]{1,0:T(2,128)(2,1)} %ngain.1, bf16[2,32,256]{2,1,0:T(8,128)(2,1)} %bitcast.4, bf16[2,32,256]{2,1,0:T(8,128)(2,1)} %bitcast.5, ...), custom_call_target="tpu_custom_call" | custom-call | tf_op jit(solution)/shard_map/retention_step/pallas_call | solution.py:455
  68.2 0.6 copy.14
  68.7 0.8 %copy.15 = f32[2,16,32,128]{3,2,1,0:T(8,128)} copy(f32[2,16,32,128]{3,2,1,0:T(8,128)S(1)} %get-tuple-element.3) | data formatting | bytes 1048576

commit v5 on v4

--- a/solution.py
+++ b/solution.py
@@ -386,7 +386,7 @@
                 ref[j, d] = term[ROWS * j : ROWS * j + ROWS].astype(bf16)
 
     def push_last(src_of, dst, sem_id):
-        for peer in dp_peers:
+        for peer in dp_peers[::-1]:
             for j in range(ROWS):
                 push(src_of(j, peer), dst, sem_id, ROWS * dp + j, peer)
         for j in range(ROWS):

time: 69.7 us -> 69.4 us (level)
  no operation moved by 1% of the time
where the time goes in v5:
time: 69.4 us; the launch traced here: 69.2 us
  Pallas kernels  67.2 us (97%)
  local copies, waits for them, and re-layouts  1.37 us (2%)
    pallas_call x1, Pallas kernels, body(): pl.pallas_call(kernel, out_shape=(vmem((ROWS, FEATS), bf16), vmem(states....  67.2 us

profile of v5, /device:TPU:1, one launch (start us, length us, event | category | flops | bytes accessed | tf_op | source)
XLA Modules:
  0.0 69.2 jit_solution(16339252032839733536)
XLA Ops:
  0.6 67.2 %retention_step.1 = (bf16[4,256]{1,0:T(4,128)(2,1)S(1)}, f32[2,16,32,128]{3,2,1,0:T(8,128)S(1)}) custom-call(bf16[4,256]{1,0:T(4,128)(2,1)} %tok.1, s32[16]{0:T(128)} %lens.1, f32[2,16,32,128]{3,2,1,0:T(8,128)} %states.1, bf16[2,256]{1,0:T(2,128)(2,1)} %ngain.1, bf16[2,32,256]{2,1,0:T(8,128)(2,1)} %bitcast.4, bf16[2,32,256]{2,1,0:T(8,128)(2,1)} %bitcast.5, ...), custom_call_target="tpu_custom_call" | custom-call | tf_op jit(solution)/shard_map/retention_step/pallas_call | solution.py:455
  67.9 0.6 copy.14
  68.4 0.8 %copy.15 = f32[2,16,32,128]{3,2,1,0:T(8,128)} copy(f32[2,16,32,128]{3,2,1,0:T(8,128)S(1)} %get-tuple-element.3) | data formatting | bytes 1048576
